TPU v7x, 32 devices: a whole 2x2x4 slice. The times are simulated.
32 devices in a mesh: ep: 4 (over y, x), tp: 8 (over z, core).
Axes of the slice: x: 2, y: 2, z: 4, core: 2. Of those that a mesh axis runs over, the one named last changes fastest.
Arguments:
- tokens: bfloat16 [1024, 2048], P('ep'), may hold values from -6 to 6
- cotangent: bfloat16 [1024, 2048], P('ep'), may hold values from -6 to 6
- group_prob: float32 [1024], P('ep'), may hold values from 0.25 to 1
- expert_prob: float32 [1024, 2], P('ep'), may hold values from 0.1 to 1
- routing: int32 [1024, 2], P('ep'), may hold values from 0 to 3, all different within a row; in each aligned block of 256 rows (0 to 255, 256 to 511, ...) at most 192 rows name the same one
- gate_weight: bfloat16 [4, 2048, 4096], P('ep', None, 'tp'), may hold values from -0.125 to 0.125
- up_weight: bfloat16 [4, 2048, 4096], P('ep', None, 'tp'), may hold values from -0.125 to 0.125
- down_weight: bfloat16 [4, 4096, 2048], P('ep', 'tp'), may hold values from -1 to 1
Outputs:
- token_grad: bfloat16 [1024, 2048], P('ep')
- group_prob_grad: float32 [1024], P('ep')
- expert_prob_grad: float32 [1024, 2], P('ep')
- gate_weight_grad: bfloat16 [4, 2048, 4096], P('ep', None, 'tp')
- up_weight_grad: bfloat16 [4, 2048, 4096], P('ep', None, 'tp')
- down_weight_grad: bfloat16 [4, 4096, 2048], P('ep', 'tp')
- gate_row_norms: float32 [4, 2048], P('ep')
- up_row_norms: float32 [4, 2048], P('ep')
- down_row_norms: float32 [4, 4096], P('ep', 'tp')
Inputs may be any that keep to these rules, and one draw needn't show every extreme that they name: `routing`: each row names 2 different experts. In each aligned block of 256 rows no expert is named by more than 192 rows, and in every draw some expert is named by exactly 192 rows of some block.
All inputs are finite; a program needn't handle non-finite values.
Results may differ from a plain program's by a relative error of at most 0.0065.
Values may be sent and summed in bfloat16 or wider, within the bound.
A program may use at most 64 MiB of HBM per device.

v0:
```python
import functools
import jax
import jax.numpy as jnp
from jax import lax
from jax.experimental import pallas as pl
from jax.experimental.pallas import tpu as pltpu
from jax.sharding import PartitionSpec as P

MESH = pl.DeviceIdType.MESH
CHUNKS = 8
DIRECT = 5


def dispatch_kernel(n_ep, mine_ref, out_ref, local_sem, send_sem, recv_sem, fwd_send, fwd_recv, z_send, z_recv):
    me = lax.axis_index("ep")
    t = lax.axis_index("tp")
    core = lax.rem(t, 2)
    partner = t + 1 - 2 * core
    side_z = lax.rem(t // 2, 2)
    across = t + 2 - 4 * side_z
    width = mine_ref.shape[2] // CHUNKS
    barrier = pltpu.get_barrier_semaphore()
    for d in range(1, n_ep):
        pl.semaphore_signal(
            barrier, inc=1, device_id={"ep": lax.rem(me + d, n_ep)}, device_id_type=MESH
        )
    pl.semaphore_signal(barrier, inc=1, device_id={"tp": partner}, device_id_type=MESH)
    pl.semaphore_signal(barrier, inc=1, device_id={"tp": across}, device_id_type=MESH)
    pl.semaphore_wait(barrier, n_ep + 1)

    def cols(c):
        j, side = (c, side_z) if c < DIRECT else (c - DIRECT, 1 - side_z)
        at = j + side * (CHUNKS - 1 - 2 * j)
        return pl.ds(pl.multiple_of(at * width, 128), width)

    def to_peer(d, c):
        dst = lax.rem(me + d, n_ep)
        return pltpu.make_async_remote_copy(
            src_ref=mine_ref.at[dst, :, cols(c)],
            dst_ref=out_ref.at[core, me, :, cols(c)],
            send_sem=send_sem.at[d, c],
            recv_sem=recv_sem.at[d, c],
            device_id={"ep": dst},
            device_id_type=MESH,
        )

    def from_peer(d, c):
        src = lax.rem(me - d + n_ep, n_ep)
        return pltpu.make_async_remote_copy(
            src_ref=mine_ref.at[me, :, cols(c)],
            dst_ref=out_ref.at[core, src, :, cols(c)],
            send_sem=send_sem.at[d, c],
            recv_sem=recv_sem.at[d, c],
            device_id={"ep": src},
            device_id_type=MESH,
        )

    def forward(d, c, side):
        src = lax.rem(me - d + n_ep, n_ep)
        source = mine_ref.at[me, :, cols(c)] if d == 0 else out_ref.at[side, src, :, cols(c)]
        return pltpu.make_async_remote_copy(
            src_ref=source,
            dst_ref=out_ref.at[side, src, :, cols(c)],
            send_sem=fwd_send.at[d, c],
            recv_sem=fwd_recv.at[d, c],
            device_id={"tp": partner},
            device_id_type=MESH,
        )

    def swap(d, c, arriving):
        src = lax.rem(me - d + n_ep, n_ep)
        ref = out_ref.at[core, src, :, cols(c + DIRECT if arriving else c)]
        return pltpu.make_async_remote_copy(
            src_ref=ref,
            dst_ref=ref,
            send_sem=z_send.at[d, c],
            recv_sem=z_recv.at[d, c],
            device_id={"tp": across},
            device_id_type=MESH,
        )

    order = sorted(range(1, n_ep), key=lambda d: abs(d - n_ep // 2))
    extra = CHUNKS - DIRECT
    for c in range(DIRECT):
        for d in order:
            to_peer(d, c).start()
    keep = pltpu.make_async_copy(mine_ref.at[me], out_ref.at[core, me], local_sem)
    keep.start()
    for c in range(CHUNKS):
        forward(0, c, core).start()
    lag = DIRECT - extra
    for c in range(DIRECT):
        for d in order:
            from_peer(d, c).wait_recv()
            if c < extra:
                swap(d, c, False).start()
            forward(d, c, core).start()
        if c >= lag:
            for d in order:
                swap(d, c - lag, True).wait_recv()
                forward(d, c - lag + DIRECT, core).start()
    keep.wait()
    for c in range(DIRECT):
        for d in order:
            to_peer(d, c).wait_send()
    for c in range(extra):
        for d in order:
            swap(d, c, False).wait_send()
    for d in range(n_ep):
        for c in range(CHUNKS):
            forward(d, c, core).wait_send()
            forward(d, c, 1 - core).wait_recv()


def dispatch(mine, n_ep):
    return pl.pallas_call(
        functools.partial(dispatch_kernel, n_ep),
        out_shape=jax.ShapeDtypeStruct((2,) + mine.shape, mine.dtype),
        in_specs=[pl.BlockSpec(memory_space=pltpu.VMEM)],
        out_specs=pl.BlockSpec(memory_space=pl.ANY),
        scratch_shapes=[
            pltpu.SemaphoreType.DMA,
            pltpu.SemaphoreType.DMA((n_ep, CHUNKS)),
            pltpu.SemaphoreType.DMA((n_ep, CHUNKS)),
            pltpu.SemaphoreType.DMA((n_ep, CHUNKS)),
            pltpu.SemaphoreType.DMA((n_ep, CHUNKS)),
            pltpu.SemaphoreType.DMA((n_ep, CHUNKS)),
            pltpu.SemaphoreType.DMA((n_ep, CHUNKS)),
        ],
        compiler_params=pltpu.CompilerParams(collective_id=0, has_side_effects=True),
        name="dispatch",
    )(mine)


def sums_kernel(n_ep, n_tp, part_ref, norm_ref, score_ref, slots, total, send_sem, recv_sem, s_send, s_recv):
    me = lax.axis_index("ep")
    t = lax.axis_index("tp")
    barrier = pltpu.get_barrier_semaphore()
    for d in range(1, n_tp):
        pl.semaphore_signal(
            barrier, inc=1, device_id={"tp": lax.rem(t + d, n_tp)}, device_id_type=MESH
        )
    for d in range(1, n_ep):
        pl.semaphore_signal(
            barrier, inc=1, device_id={"ep": lax.rem(me + d, n_ep)}, device_id_type=MESH
        )
    pl.semaphore_wait(barrier, n_tp - 1 + n_ep - 1)

    def part_to(d):
        return pltpu.make_async_remote_copy(
            src_ref=part_ref,
            dst_ref=slots.at[t],
            send_sem=send_sem.at[d],
            recv_sem=recv_sem.at[d],
            device_id={"tp": lax.rem(t + d, n_tp)},
            device_id_type=MESH,
        )

    def part_from(d):
        src = lax.rem(t - d + n_tp, n_tp)
        return pltpu.make_async_remote_copy(
            src_ref=part_ref,
            dst_ref=slots.at[src],
            send_sem=send_sem.at[d],
            recv_sem=recv_sem.at[d],
            device_id={"tp": src},
            device_id_type=MESH,
        )

    for d in range(1, n_tp):
        part_to(d).start()
    slots[t] = part_ref[...]
    for d in range(1, n_tp):
        part_from(d).wait_recv()
    acc = slots[0]
    for i in range(1, n_tp):
        acc = acc + slots[i]
    total[...] = acc
    rows = 8 * n_ep

    def score_to(d):
        dst = lax.rem(me + d, n_ep)
        return pltpu.make_async_remote_copy(
            src_ref=total.at[pl.ds(pl.multiple_of(dst * 8, 8), 8)],
            dst_ref=score_ref.at[me],
            send_sem=s_send.at[d],
            recv_sem=s_recv.at[d],
            device_id={"ep": dst},
            device_id_type=MESH,
        )

    def score_from(d):
        src = lax.rem(me - d + n_ep, n_ep)
        return pltpu.make_async_remote_copy(
            src_ref=total.at[pl.ds(0, 8)],
            dst_ref=score_ref.at[src],
            send_sem=s_send.at[d],
            recv_sem=s_recv.at[d],
            device_id={"ep": src},
            device_id_type=MESH,
        )

    norm_ref[...] = acc[rows:]
    for d in range(1, n_tp):
        part_to(d).wait_send()
    for d in range(1, n_ep):
        score_to(d).start()
    score_ref[me] = total[pl.ds(pl.multiple_of(me * 8, 8), 8)]
    for d in range(1, n_ep):
        score_from(d).wait_recv()
    for d in range(1, n_ep):
        score_to(d).wait_send()


def small_sums(scores, norms, n_ep, n_tp):
    cap = scores.shape[1]
    width = norms.shape[1]
    padded = jnp.pad(scores, ((0, 0), (0, 1024 - cap))).reshape(n_ep * 8, 128)
    part = jnp.concatenate([padded, norms.reshape(2 * width // 128, 128)], axis=0)
    norm_out, score_out = pl.pallas_call(
        functools.partial(sums_kernel, n_ep, n_tp),
        out_shape=(
            jax.ShapeDtypeStruct((2 * width // 128, 128), jnp.float32),
            jax.ShapeDtypeStruct((n_ep, 8, 128), jnp.float32),
        ),
        in_specs=[pl.BlockSpec(memory_space=pltpu.VMEM)],
        out_specs=(
            pl.BlockSpec(memory_space=pltpu.VMEM),
            pl.BlockSpec(memory_space=pltpu.VMEM),
        ),
        scratch_shapes=[
            pltpu.VMEM((n_tp,) + part.shape, jnp.float32),
            pltpu.VMEM(part.shape, jnp.float32),
            pltpu.SemaphoreType.DMA((n_tp,)),
            pltpu.SemaphoreType.DMA((n_tp,)),
            pltpu.SemaphoreType.DMA((n_ep,)),
            pltpu.SemaphoreType.DMA((n_ep,)),
        ],
        compiler_params=pltpu.CompilerParams(collective_id=1, has_side_effects=True),
        cost_estimate=pl.CostEstimate(flops=0, bytes_accessed=20_000_000, transcendentals=0),
        name="small_sums",
    )(part)
    return score_out.reshape(n_ep, 1024)[:, :cap], norm_out.reshape(2, width)


def finish_kernel(
    n_ep, n_tp, both_ref, gate_ref, up_ref, hid_ref, part_ref, score_ref, pick_ref,
    out_ref, gate_out, up_out, down_out, norm_ref, down_norm_ref, score_out,
    rows_in, rows_scaled, gate_v, up_v, hid_v, gate_g, up_g, down_g, norm_part,
    s_slots, s_total, n_slots, bufs, accs, returned,
    load_sem, store_sem, rs_send, rs_recv, ep_send, ep_recv, ag_send, ag_recv,
    sc_send, sc_recv, sx_send, sx_recv, nm_send, nm_recv,
):
    me = lax.axis_index("ep")
    t = lax.axis_index("tp")
    cap, width = part_ref.shape[1], part_ref.shape[2]
    ff = gate_v.shape[1]
    tok = out_ref.shape[0]
    levels = len(bufs)
    bits = [lax.rem(t // (1 << s), 2) for s in range(levels)]
    peers = [t + (1 - 2 * bits[s]) * (1 << s) for s in range(levels)]

    def remote(src, dst, send, recv, device):
        return pltpu.make_async_remote_copy(
            src_ref=src, dst_ref=dst, send_sem=send, recv_sem=recv,
            device_id=device, device_id_type=MESH,
        )

    loads = []
    for b in range(n_ep):
        loads.append(pltpu.make_async_copy(
            both_ref.at[0, b], rows_in.at[pl.ds(b * cap, cap)], load_sem.at[len(loads)]))
        loads.append(pltpu.make_async_copy(
            both_ref.at[1, b], rows_scaled.at[pl.ds(b * cap, cap)], load_sem.at[len(loads)]))
    for src, dst in ((gate_ref, gate_v), (up_ref, up_v), (hid_ref, hid_v)):
        loads.append(pltpu.make_async_copy(src, dst, load_sem.at[len(loads)]))

    barrier = pltpu.get_barrier_semaphore()
    for d in range(1, n_tp):
        pl.semaphore_signal(
            barrier, inc=1, device_id={"tp": lax.rem(t + d, n_tp)}, device_id_type=MESH
        )
    for d in range(1, n_ep):
        pl.semaphore_signal(
            barrier, inc=1, device_id={"ep": lax.rem(me + d, n_ep)}, device_id_type=MESH
        )
    pl.semaphore_wait(barrier, n_tp - 1 + n_ep - 1)

    order = sorted(range(1, n_ep), key=lambda d: abs(d - n_ep // 2)) + [0]

    def block(i):
        return lax.rem(me + order[i], n_ep)

    def halves(s):
        w = width >> (s + 1)
        keep = pl.ds(pl.multiple_of(bits[s] * w, 128), w)
        give = pl.ds(pl.multiple_of((1 - bits[s]) * w, 128), w)
        return keep, give

    def exchange(s, i):
        _, give = halves(s)
        src = part_ref.at[block(i), :, give] if s == 0 else accs[s - 1].at[i, :, give]
        return remote(src, bufs[s].at[i], rs_send.at[s, i], rs_recv.at[s, i], {"tp": peers[s]})

    def to_owner(i):
        d = order[i]
        return remote(
            accs[levels - 1].at[i],
            returned.at[pl.ds(pl.multiple_of(me * cap, 16), cap)],
            ep_send.at[d], ep_recv.at[d], {"ep": block(i)},
        )

    def from_owner(d):
        src = lax.rem(me - d + n_ep, n_ep)
        return remote(
            accs[levels - 1].at[0],
            returned.at[pl.ds(pl.multiple_of(src * cap, 16), cap)],
            ep_send.at[d], ep_recv.at[d], {"ep": src},
        )

    def score_to(d):
        return remote(score_ref, s_slots.at[t], sc_send.at[d], sc_recv.at[d],
                      {"tp": lax.rem(t + d, n_tp)})

    def score_from(d):
        src = lax.rem(t - d + n_tp, n_tp)
        return remote(score_ref, s_slots.at[src], sc_send.at[d], sc_recv.at[d], {"tp": src})

    def norm_to(d):
        return remote(norm_part, n_slots.at[t], nm_send.at[d], nm_recv.at[d],
                      {"tp": lax.rem(t + d, n_tp)})

    def norm_from(d):
        src = lax.rem(t - d + n_tp, n_tp)
        return remote(norm_part, n_slots.at[src], nm_send.at[d], nm_recv.at[d], {"tp": src})

    def score_back(d):
        dst = lax.rem(me + d, n_ep)
        return remote(s_total.at[pl.ds(pl.multiple_of(dst * 8, 8), 8)], score_out.at[me],
                      sx_send.at[d], sx_recv.at[d], {"ep": dst})

    def score_arrive(d):
        src = lax.rem(me - d + n_ep, n_ep)
        return remote(s_total.at[pl.ds(0, 8)], score_out.at[src],
                      sx_send.at[d], sx_recv.at[d], {"ep": src})

    for i in range(n_ep):
        exchange(0, i).start()
    for d in range(1, n_tp):
        score_to(d).start()
    for copy in loads:
        copy.start()
    s_slots[t] = score_ref[...]

    rows = (((0,), (0,)), ((), ()))
    step = 256
    half = width // step // 2

    def fold(sq):
        parts = [sq[:, j * 128:(j + 1) * 128] for j in range(sq.shape[1] // 128)]
        return functools.reduce(jnp.add, parts)

    def line(x):
        return jnp.sum(jnp.transpose(x), axis=0, keepdims=True)

    def gate_up(first):
        def body(j, carry):
            at = pl.ds(pl.multiple_of(j * step, step), step)
            lhs = rows_in[:, at]
            for n, (rhs, out) in enumerate(((gate_v, gate_g), (up_v, up_g))):
                total = lax.dot_general(lhs, rhs[...], rows, preferred_element_type=jnp.float32)
                out[at, :] = total.astype(jnp.bfloat16)
                sq = fold(total * total)
                for h in range(step // 128):
                    norm_part[n, pl.ds(j * (step // 128) + h, 1), :] = line(
                        sq[h * 128:(h + 1) * 128]
                    ) / (ff * n_tp)
            return carry
        lax.fori_loop(first, first + half, body, 0)

    def down():
        def body(j, carry):
            at = pl.ds(pl.multiple_of(j * step, step), step)
            lhs = hid_v[:, at]
            sq = None
            for c in range(0, width, 512):
                total = lax.dot_general(
                    lhs, rows_scaled[:, c:c + 512], rows, preferred_element_type=jnp.float32
                )
                down_g[at, c:c + 512] = total.astype(jnp.bfloat16)
                more = fold(total * total)
                sq = more if sq is None else sq + more
            for h in range(step // 128):
                down_norm_ref[pl.ds(j * (step // 128) + h, 1), :] = line(
                    sq[h * 128:(h + 1) * 128]
                ) / width
            return carry
        lax.fori_loop(0, ff // step, body, 0)

    stores = [
        pltpu.make_async_copy(a, b, store_sem.at[n])
        for n, (a, b) in enumerate(((gate_g, gate_out), (up_g, up_out), (down_g, down_out)))
    ]

    def work_first():
        for copy in loads:
            copy.wait()
        gate_up(0)

    def work_second():
        gate_up(half)
        for d in range(1, n_tp):
            norm_to(d).start()
        n_slots[t] = norm_part[...]
        stores[0].start()
        stores[1].start()

    def work_third():
        for d in range(1, n_tp):
            score_from(d).wait_recv()
        acc = s_slots[0]
        for i in range(1, n_tp):
            acc = acc + s_slots[i]
        s_total[...] = acc
        down()
        stores[2].start()
        for d in range(1, n_ep):
            score_back(d).start()
        score_out[me] = s_total[pl.ds(pl.multiple_of(me * 8, 8), 8)]

    work = [work_first, work_second, work_third]
    for tick in range(max(n_ep + levels - 1, len(work))):
        for i in range(n_ep):
            s = tick - i
            if not 0 <= s < levels:
                continue
            exchange(s, i).wait_recv()
            keep, _ = halves(s)
            own = part_ref[block(i), :, keep] if s == 0 else accs[s - 1][i, :, keep]
            total = own.astype(jnp.float32) + bufs[s][i].astype(jnp.float32)
            accs[s][i] = total.astype(jnp.bfloat16)
            if s + 1 < levels:
                exchange(s + 1, i).start()
            elif order[i]:
                to_owner(i).start()
            else:
                returned[pl.ds(pl.multiple_of(me * cap, 16), cap), :] = total.astype(jnp.bfloat16)
        if tick < len(work):
            work[tick]()

    for d in range(1, n_ep):
        from_owner(d).wait_recv()
    share = width >> levels
    base = [None] * (levels + 1)
    base[0] = 0
    for s in range(levels):
        base[s + 1] = base[s] + bits[s] * (width >> (s + 1))
    pieces = 2
    piece = tok // pieces

    def spread(s, p):
        w = width >> (s + 1)
        at = pl.ds(pl.multiple_of(base[s + 1], 128), w)
        ref = out_ref.at[pl.ds(p * piece, piece), at]
        return remote(ref, ref, ag_send.at[s, p], ag_recv.at[s, p], {"tp": peers[s]})

    def arrived(s, p):
        w = width >> (s + 1)
        at = pl.ds(pl.multiple_of(base[s] + (1 - bits[s]) * w, 128), w)
        ref = out_ref.at[pl.ds(p * piece, piece), at]
        return remote(ref, ref, ag_send.at[s, p], ag_recv.at[s, p], {"tp": peers[s]})

    for p in range(pieces):
        grad = jnp.dot(
            pick_ref[p * piece:(p + 1) * piece, :], returned[...],
            preferred_element_type=jnp.float32,
        )
        out_ref[p * piece:(p + 1) * piece, pl.ds(pl.multiple_of(base[levels], 128), share)] = (
            grad.astype(jnp.bfloat16)
        )
        spread(levels - 1, p).start()
    for d in range(1, n_tp):
        norm_from(d).wait_recv()
    acc = n_slots[0]
    for i in range(1, n_tp):
        acc = acc + n_slots[i]
    norm_ref[...] = acc
    for s in reversed(range(levels)):
        for p in range(pieces):
            arrived(s, p).wait_recv()
            if s:
                spread(s - 1, p).start()

    for d in range(1, n_ep):
        score_arrive(d).wait_recv()
        score_back(d).wait_send()
    for i in range(n_ep):
        for s in range(levels):
            exchange(s, i).wait_send()
        if order[i]:
            to_owner(i).wait_send()
    for d in range(1, n_tp):
        score_to(d).wait_send()
        norm_to(d).wait_send()
    for s in range(levels):
        for p in range(pieces):
            spread(s, p).wait_send()
    for copy in stores:
        copy.wait()


def finish(both, gate_pre, up_pre, hidden, part, score_part, pick_t, n_ep, n_tp):
    cap, width = part.shape[1:]
    rows, ff = gate_pre.shape
    tok = pick_t.shape[0]
    levels = n_tp.bit_length() - 1
    scores = jnp.pad(score_part, ((0, 0), (0, 1024 - cap))).reshape(n_ep * 8, 128)
    bf, f32 = jnp.bfloat16, jnp.float32
    vmem = pl.BlockSpec(memory_space=pltpu.VMEM)
    hbm = pl.BlockSpec(memory_space=pl.ANY)
    dma = pltpu.SemaphoreType.DMA
    stages = [pltpu.VMEM((n_ep, cap, width >> (s + 1)), bf) for s in range(levels)]
    outs = pl.pallas_call(
        functools.partial(finish_kernel, n_ep, n_tp),
        out_shape=(
            jax.ShapeDtypeStruct((tok, width), bf),
            jax.ShapeDtypeStruct((width, ff), bf),
            jax.ShapeDtypeStruct((width, ff), bf),
            jax.ShapeDtypeStruct((ff, width), bf),
            jax.ShapeDtypeStruct((2, width // 128, 128), f32),
            jax.ShapeDtypeStruct((ff // 128, 128), f32),
            jax.ShapeDtypeStruct((n_ep, 8, 128), f32),
        ),
        in_specs=[hbm, hbm, hbm, hbm, vmem, vmem, vmem],
        out_specs=(vmem, hbm, hbm, hbm, vmem, vmem, vmem),
        scratch_shapes=[
            pltpu.VMEM((rows, width), bf),
            pltpu.VMEM((rows, width), bf),
            pltpu.VMEM((rows, ff), bf),
            pltpu.VMEM((rows, ff), bf),
            pltpu.VMEM((rows, ff), bf),
            pltpu.VMEM((width, ff), bf),
            pltpu.VMEM((width, ff), bf),
            pltpu.VMEM((ff, width), bf),
            pltpu.VMEM((2, width // 128, 128), f32),
            pltpu.VMEM((n_tp,) + scores.shape, f32),
            pltpu.VMEM(scores.shape, f32),
            pltpu.VMEM((n_tp, 2, width // 128, 128), f32),
            list(stages),
            list(stages),
            pltpu.VMEM((rows, width >> levels), bf),
            dma((2 * n_ep + 3,)),
            dma((3,)),
            dma((levels, n_ep)),
            dma((levels, n_ep)),
            dma((n_ep,)),
            dma((n_ep,)),
            dma((levels, 2)),
            dma((levels, 2)),
            dma((n_tp,)),
            dma((n_tp,)),
            dma((n_ep,)),
            dma((n_ep,)),
            dma((n_tp,)),
            dma((n_tp,)),
        ],
        compiler_params=pltpu.CompilerParams(
            collective_id=2, has_side_effects=True, vmem_limit_bytes=48 << 20
        ),
        name="finish",
    )(both, gate_pre, up_pre, hidden, part, scores, pick_t)
    token_grad, gate_g, up_g, down_g, norms, down_norms, score_out = outs
    return (
        token_grad, gate_g, up_g, down_g, norms.reshape(2, width),
        down_norms.reshape(ff), score_out.reshape(n_ep, 1024)[:, :cap],
    )


def local(tokens, cotangent, group_prob, expert_prob, routing, gate_weight, up_weight, down_weight):
    tok_count, model_width = tokens.shape
    top_count = routing.shape[1]
    n_ep = lax.axis_size("ep")
    n_tp = lax.axis_size("tp")
    capacity = 3 * tok_count * top_count // (2 * n_ep)
    buffer_rows = n_ep * capacity
    core = lax.rem(lax.axis_index("tp"), 2)
    weight = group_prob[:, None] * expert_prob

    experts = jnp.arange(n_ep, dtype=jnp.int32)[:, None]
    picks = [routing[None, :, k] == experts for k in range(top_count)]
    named = functools.reduce(jnp.logical_or, picks)
    weight_of = sum(jnp.where(picks[k], weight[None, :, k], 0.0) for k in range(top_count))
    earlier = (
        lax.broadcasted_iota(jnp.int32, (tok_count, tok_count), 0)
        < lax.broadcasted_iota(jnp.int32, (tok_count, tok_count), 1)
    ).astype(jnp.bfloat16)
    before = jnp.dot(named.astype(jnp.bfloat16), earlier, preferred_element_type=jnp.float32)
    place = jnp.where(named, before.astype(jnp.int32), -1)
    filled = place[:, None, :] == lax.broadcasted_iota(jnp.int32, (n_ep, capacity, tok_count), 1)
    pick = filled.astype(jnp.bfloat16).reshape(buffer_rows, tok_count)
    slot_weight = jnp.sum(jnp.where(filled, weight_of[:, None, :], 0.0), axis=2).reshape(buffer_rows, 1)

    source = jnp.where(core == 0, tokens, cotangent)
    factor = jnp.where(core == 0, 1.0, slot_weight)
    mine = jnp.dot(pick, source, preferred_element_type=jnp.float32) * factor
    mine = mine.astype(jnp.bfloat16).reshape(n_ep, capacity, model_width)
    both = dispatch(mine, n_ep)
    flat_in = both[0].reshape(buffer_rows, model_width)
    flat_scaled = both[1].reshape(buffer_rows, model_width)

    w_gate = gate_weight[0]
    w_up = up_weight[0]
    w_down = down_weight[0]
    hidden_total = gate_weight.shape[2] * n_tp
    contract_last = (((1,), (1,)), ((), ()))
    contract_rows = (((0,), (0,)), ((), ()))
    pre_gate = jnp.dot(flat_in, w_gate, preferred_element_type=jnp.float32)
    pre_up = jnp.dot(flat_in, w_up, preferred_element_type=jnp.float32)
    sigma = jax.nn.sigmoid(pre_gate)
    activated = pre_gate * sigma
    derivative = sigma * (1.0 + pre_gate * (1.0 - sigma))
    hidden = (activated * pre_up).astype(jnp.bfloat16)
    hidden_grad = lax.dot_general(
        flat_scaled, w_down, contract_last, preferred_element_type=jnp.float32
    )
    score_part = jnp.sum(hidden.astype(jnp.float32) * hidden_grad, axis=1).reshape(n_ep, capacity)
    gate_pre = (hidden_grad * pre_up * derivative).astype(jnp.bfloat16)
    up_pre = (hidden_grad * activated).astype(jnp.bfloat16)
    input_part = lax.dot_general(
        gate_pre, w_gate, contract_last, preferred_element_type=jnp.float32
    )
    input_part = input_part + lax.dot_general(
        up_pre, w_up, contract_last, preferred_element_type=jnp.float32
    )
    input_part = input_part.astype(jnp.bfloat16).reshape(n_ep, capacity, model_width)
    if n_tp & (n_tp - 1) == 0 and model_width // n_tp % 128 == 0:
        pick_t = pick.T
        token_grad, gate_grad, up_grad, down_grad, row_norms, down_norms, scores = finish(
            both, gate_pre, up_pre, hidden, input_part, score_part, pick_t, n_ep, n_tp
        )
    else:
        share = lax.psum_scatter(input_part, "tp", scatter_dimension=2, tiled=True)

        down_sum = lax.dot_general(
            hidden, flat_scaled, contract_rows, preferred_element_type=jnp.float32
        )
        gate_sum = lax.dot_general(flat_in, gate_pre, contract_rows, preferred_element_type=jnp.float32)
        up_sum = lax.dot_general(flat_in, up_pre, contract_rows, preferred_element_type=jnp.float32)
        norm_part = (
            jnp.stack([jnp.sum(gate_sum * gate_sum, axis=1), jnp.sum(up_sum * up_sum, axis=1)])
            / hidden_total
        )
        down_norms = jnp.sum(down_sum * down_sum, axis=1) / model_width
        scores, row_norms = small_sums(score_part, norm_part, n_ep, n_tp)

        share, scores, row_norms, down_norms = lax.optimization_barrier(
            (share, scores, row_norms, down_norms)
        )
        returned = lax.all_to_all(share, "ep", split_axis=0, concat_axis=0, tiled=True)
        returned = returned.reshape(buffer_rows, -1)
        token_share = lax.dot_general(pick, returned, contract_rows, preferred_element_type=jnp.float32)
        token_grad = lax.all_gather(token_share.astype(jnp.bfloat16), "tp", axis=1, tiled=True)
        gate_grad, up_grad, down_grad = (
            x.astype(jnp.bfloat16) for x in (gate_sum, up_sum, down_sum)
        )

    score_of = jnp.sum(jnp.where(filled, scores[:, :, None], 0.0), axis=1)
    slot_score = jnp.stack(
        [jnp.sum(jnp.where(p, score_of, 0.0), axis=0) for p in picks], axis=1
    ) / weight
    expert_prob_grad = group_prob[:, None] * slot_score
    group_prob_grad = jnp.sum(expert_prob * slot_score, axis=1)
    return (
        token_grad,
        group_prob_grad,
        expert_prob_grad,
        gate_grad[None],
        up_grad[None],
        down_grad[None],
        row_norms[0][None],
        row_norms[1][None],
        down_norms[None],
    )


def solution(mesh):
    return jax.shard_map(
        local,
        mesh=mesh,
        in_specs=(
            P("ep", None),
            P("ep", None),
            P("ep"),
            P("ep", None),
            P("ep", None),
            P("ep", None, "tp"),
            P("ep", None, "tp"),
            P("ep", "tp", None),
        ),
        out_specs=(
            P("ep", None),
            P("ep"),
            P("ep", None),
            P("ep", None, "tp"),
            P("ep", None, "tp"),
            P("ep", "tp", None),
            P("ep", None),
            P("ep", None),
            P("ep", "tp"),
        ),
        check_vma=False,
    )
```

profile of v0, /device:TPU:0, one launch (start us, length us, event | category | flops | bytes accessed | tf_op | source)
XLA Modules:
  0.0 126.7 jit_solution(17676445336937179044)
XLA Ops:
  0.6 0.0 copy-start
  0.7 0.8 broadcast_multiply_fusion.1
  1.5 0.8 fusion.20
  2.3 0.2 fusion.10
  2.4 0.2 select_reduce_fusion.1
  2.7 0.1 select_n.66
  2.8 0.1 iota.40
  2.8 0.1 eq.64
  2.9 1.1 copy.27
  4.1 1.3 %convert_bitcast_fusion = (bf16[256,768]{1,0:T(8,128)(2,1)S(1)}, pred[768,256]{0,1:T(32,128)(4,1)S(1)}) fusion(s32[768,256]{0,1:T(8,128)} %copy.27, s32[768]{0:T(1024)S(1)} %iota.40), kind=kLoop, calls=%fused_computation.24 | loop fusion | flops 393216 | bytes 1379328 | tf_op jit(solution)/shard_map/transpose | solution.py:637
  5.3 4.0 %multiply_convert_fusion = bf16[768,2048]{1,0:T(8,128)(2,1)} fusion(pred[768,256]{0,1:T(32,128)(4,1)S(1)} %get-tuple-element.28, f32[768]{0:T(1024)S(1)} %select_n.66, bf16[256,2048]{1,0:T(8,128)(2,1)} %param.8, bf16[256,2048]{1,0:T(8,128)(2,1)} %param.9, pred[]{:T(512)S(6)} %eq.67), kind=kOutput, calls=%fused_computation.1 | convolution fusion | flops 808976384 | bytes 5442561 | tf_op jit(solution)/shard_map/dot_general | solution.py:605
  9.3 35.4 %dispatch.1.both_ref = bf16[2,4,192,2048]{3,2,1,0:T(8,128)(2,1)} custom-call(bf16[4,192,2048]{2,1,0:T(8,128)(2,1)} %bitcast.50), custom_call_target="tpu_custom_call" | custom-call | tf_op jit(solution)/shard_map/dispatch/pallas_call | solution.py:116
  44.8 3.4 %fusion.17 = (bf16[1,4,192,2048]{3,2,1,0:T(8,128)(2,1)S(1)}, bf16[1,4,192,2048]{3,2,1,0:T(8,128)(2,1)S(1)}) fusion(bf16[2,4,192,2048]{3,2,1,0:T(8,128)(2,1)} %dispatch.1.both_ref), kind=kLoop, calls=%fused_computation.41 | loop fusion | bytes 12582912 | tf_op jit(solution)/shard_map/slice | solution.py:609
  48.2 0.0 copy-done
  48.2 0.0 copy-start.5
  48.2 1.8 %fusion.2 = f32[768,512]{1,0:T(8,128)S(1)} fusion(bf16[768,2048]{1,0:T(8,128)(2,1)S(1)} %bitcast.51, bf16[1,2048,512]{2,1,0:T(8,128)(2,1)S(1)} %copy-done), kind=kOutput, calls=%fused_computation.4 | convolution fusion | flops 1610612736 | bytes 6815744 | tf_op jit(solution)/shard_map/dot_general | solution.py:617
  50.0 0.0 copy-done.5
  50.0 0.0 copy-start.9
  50.0 1.8 %fusion.5 = f32[768,512]{1,0:T(8,128)S(1)} fusion(bf16[768,2048]{1,0:T(8,128)(2,1)S(1)} %bitcast.52, bf16[1,2048,512]{2,1,0:T(8,128)(2,1)S(1)} %copy-done.5), kind=kOutput, calls=%fused_computation.7 | convolution fusion | flops 1610612736 | bytes 6815744 | tf_op jit(solution)/shard_map/dot_general | solution.py:618
  51.8 0.0 copy-done.9
  51.8 3.6 %multiply_reduce_fusion = (f32[768]{0:T(1024)S(1)}, bf16[768,512]{1,0:T(8,128)(2,1)}, bf16[768,512]{1,0:T(8,128)(2,1)S(1)}, bf16[768,512]{1,0:T(8,128)(2,1)}) fusion(f32[768,512]{1,0:T(8,128)S(1)} %fusion.5, f32[768,512]{1,0:T(8,128)S(1)} %fusion.2, bf16[768,2048]{1,0:T(8,128)(2,1)S(1)} %bitcast.49, bf16[1,512,2048]{2,1,0:T(8,128)(2,1)S(1)} %copy-done.9), kind=kOutput, calls=%fused_computation.11 | convolution fusion | flops 1617689856 | bytes 10750976 | tf_op jit(solution)/shard_map/dot_general | solution.py:623
  55.4 0.1 reshape.128
  55.5 0.0 copy-start.1
  55.5 0.0 copy-start.6
  55.5 1.8 %fusion = f32[768,2048]{1,0:T(8,128)S(1)} fusion(bf16[768,512]{1,0:T(8,128)(2,1)S(1)} %get-tuple-element.33.gate_ref, bf16[1,2048,512]{2,1,0:T(8,128)(2,1)S(1)} %copy-done), kind=kOutput, calls=%fused_computation.2 | convolution fusion | flops 1610612736 | bytes 9175040 | tf_op jit(solution)/shard_map/dot_general | solution.py:629
  57.3 0.0 copy-done.1
  57.4 0.0 copy-done.6
  57.4 0.0 copy-start.2
  57.4 3.5 %add_convert_fusion = bf16[768,2048]{1,0:T(8,128)(2,1)} fusion(f32[768,2048]{1,0:T(8,128)S(1)} %fusion, bf16[768,512]{1,0:T(8,128)(2,1)S(1)} %copy-done.1, bf16[1,2048,512]{2,1,0:T(8,128)(2,1)S(1)} %copy-done.6), kind=kOutput, calls=%fused_computation | convolution fusion | flops 1613758464 | bytes 12320768 | tf_op jit(solution)/shard_map/dot_general | solution.py:632
  60.9 0.0 copy-done.2
  60.9 0.0 copy-start.7
  60.9 0.0 copy-start.8
  60.9 56.2 %finish.1 = (bf16[256,2048]{1,0:T(8,128)(2,1)S(1)}, bf16[2048,512]{1,0:T(8,128)(2,1)S(1)}, bf16[2048,512]{1,0:T(8,128)(2,1)}, bf16[512,2048]{1,0:T(8,128)(2,1)},...) custom-call(bf16[2,4,192,2048]{3,2,1,0:T(8,128)(2,1)} %dispatch.1.both_ref, ...), custom_call_target="tpu_custom_call" | custom-call | tf_op jit(solution)/shard_map/finish/pallas_call | solution.py:523
  117.1 0.2 select_reduce_fusion
  117.3 0.0 copy-done.7
  117.3 0.0 copy-done.8
  117.3 0.6 broadcast_multiply_fusion
  117.9 0.6 multiply_reduce_fusion.1
  118.5 0.6 fusion.18
  119.1 1.0 copy.49
  120.1 0.0 copy-start.4
  120.1 1.3 %copy.50 = bf16[1,2048,512]{2,1,0:T(8,128)(2,1)} copy(bf16[1,2048,512]{2,1,0:T(8,128)(2,1)S(1)} %bitcast.44) | data formatting | bytes 4194304
  121.4 1.0 copy-done.4
  122.4 0.0 copy-start.3
  122.4 1.3 %copy.51 = bf16[1,2048,512]{2,1,0:T(8,128)(2,1)} copy(bf16[1,2048,512]{2,1,0:T(8,128)(2,1)S(1)} %bitcast.54) | data formatting | bytes 4194304
  123.7 1.0 copy-done.3
  124.8 1.3 %copy.52 = bf16[1,512,2048]{2,1,0:T(8,128)(2,1)} copy(bf16[1,512,2048]{2,1,0:T(8,128)(2,1)S(1)} %bitcast.53) | data formatting | bytes 4194304
  126.1 0.6 copy.53
  (9 shorter events, 0.1 us)
Async XLA Ops:
  0.6 47.6 %copy-start = (bf16[1,2048,512]{2,1,0:T(8,128)(2,1)S(1)}, bf16[1,2048,512]{2,1,0:T(8,128)(2,1)}, u32[]{:S(2)}) copy-start(bf16[1,2048,512]{2,1,0:T(8,128)(2,1)} %param.13) | copy-start | bytes 6291460
  48.2 1.8 %copy-start.5 = (bf16[1,2048,512]{2,1,0:T(8,128)(2,1)S(1)}, bf16[1,2048,512]{2,1,0:T(8,128)(2,1)}, u32[]{:S(2)}) copy-start(bf16[1,2048,512]{2,1,0:T(8,128)(2,1)} %param.14) | copy-start | bytes 6291460
  50.0 1.8 %copy-start.9 = (bf16[1,512,2048]{2,1,0:T(8,128)(2,1)S(1)}, bf16[1,512,2048]{2,1,0:T(8,128)(2,1)}, u32[]{:S(2)}) copy-start(bf16[1,512,2048]{2,1,0:T(8,128)(2,1)} %param.15) | copy-start | bytes 6291460
  55.5 1.9 %copy-start.1 = (bf16[768,512]{1,0:T(8,128)(2,1)S(1)}, bf16[768,512]{1,0:T(8,128)(2,1)}, u32[]{:S(2)}) copy-start(bf16[768,512]{1,0:T(8,128)(2,1)} %get-tuple-element.34.up_ref) | copy-start | bytes 2359300
  55.5 1.9 %copy-start.6 = (bf16[1,2048,512]{2,1,0:T(8,128)(2,1)S(1)}, bf16[1,2048,512]{2,1,0:T(8,128)(2,1)}, u32[]{:S(2)}) copy-start(bf16[1,2048,512]{2,1,0:T(8,128)(2,1)} %param.14) | copy-start | bytes 6291460
  57.4 3.5 %copy-start.2 = (bf16[768,512]{1,0:T(8,128)(2,1)S(1)}, bf16[768,512]{1,0:T(8,128)(2,1)}, u32[]{:S(2)}) copy-start(bf16[768,512]{1,0:T(8,128)(2,1)} %get-tuple-element.30.hid_ref) | copy-start | bytes 2359300
  60.9 56.4 %copy-start.7 = (f32[256,2]{0,1:T(2,128)S(1)}, f32[256,2]{0,1:T(2,128)}, u32[]{:S(2)}) copy-start(f32[256,2]{0,1:T(2,128)} %param.11) | copy-start | bytes 6148
  60.9 56.4 %copy-start.8 = (f32[256]{0:T(256)S(1)}, f32[256]{0:T(256)}, u32[]{:S(2)}) copy-start(f32[256]{0:T(256)} %param.10) | copy-start | bytes 3076
  120.1 2.3 %copy-start.4 = (bf16[2048,512]{1,0:T(8,128)(2,1)S(1)}, bf16[2048,512]{1,0:T(8,128)(2,1)}, u32[]{:S(2)}) copy-start(bf16[2048,512]{1,0:T(8,128)(2,1)} %get-tuple-element.19) | copy-start | bytes 6291460
  122.4 2.3 %copy-start.3 = (bf16[512,2048]{1,0:T(8,128)(2,1)S(1)}, bf16[512,2048]{1,0:T(8,128)(2,1)}, u32[]{:S(2)}) copy-start(bf16[512,2048]{1,0:T(8,128)(2,1)} %get-tuple-element.20) | copy-start | bytes 6291460
where the time goes:
time: 127 us
  Pallas kernels  91.6 us (72%)
  matrix products  16.6 us (13%)
  local copies, waits for them, and re-layouts  13.9 us (11%)
  other arithmetic  3.74 us (3%)
    pallas_call x1, Pallas kernels, finish(): pl.pallas_call(functools.partial(finish_kernel, n_ep, n_tp), out_shape=(j...  56.2 us
    pallas_call x1, Pallas kernels, dispatch(): pl.pallas_call(functools.partial(dispatch_kernel, n_ep), out_shape=jax.Sh...  35.4 us
    unnamed x26, local copies, waits for them, and re-layouts  7.61 us
    dot_general x1, matrix products, local(): mine = jnp.dot(pick, source, preferred_element_type=jnp.float32) * factor  3.99 us
    dot_general x1, matrix products, local(): lax.dot_general(flat_scaled, w_down, contract_last, preferred_element_typ...  3.56 us
    dot_general x1, matrix products, local(): lax.dot_general(up_pre, w_up, contract_last, preferred_element_type=jnp.f...  3.52 us
    slice x1, local copies, waits for them, and re-layouts, local(): flat_scaled = both[1].reshape(buffer_rows, model_width)  3.43 us

commit v1 on v0

v1 whole, which is shorter than its diff:
```python
import functools
import jax
import jax.numpy as jnp
from jax import lax
from jax.experimental import pallas as pl
from jax.experimental.pallas import tpu as pltpu
from jax.sharding import PartitionSpec as P

MESH = pl.DeviceIdType.MESH
CHUNKS = 8
DIRECT = 5


def dispatch_kernel(n_ep, mine_ref, out_ref, local_sem, send_sem, recv_sem, fwd_send, fwd_recv, z_send, z_recv):
    me = lax.axis_index("ep")
    t = lax.axis_index("tp")
    core = lax.rem(t, 2)
    partner = t + 1 - 2 * core
    side_z = lax.rem(t // 2, 2)
    across = t + 2 - 4 * side_z
    width = mine_ref.shape[2] // CHUNKS
    barrier = pltpu.get_barrier_semaphore()
    for d in range(1, n_ep):
        pl.semaphore_signal(
            barrier, inc=1, device_id={"ep": lax.rem(me + d, n_ep)}, device_id_type=MESH
        )
    pl.semaphore_signal(barrier, inc=1, device_id={"tp": partner}, device_id_type=MESH)
    pl.semaphore_signal(barrier, inc=1, device_id={"tp": across}, device_id_type=MESH)
    pl.semaphore_wait(barrier, n_ep + 1)

    def cols(c):
        j, side = (c, side_z) if c < DIRECT else (c - DIRECT, 1 - side_z)
        at = j + side * (CHUNKS - 1 - 2 * j)
        return pl.ds(pl.multiple_of(at * width, 128), width)

    def to_peer(d, c):
        dst = lax.rem(me + d, n_ep)
        return pltpu.make_async_remote_copy(
            src_ref=mine_ref.at[dst, :, cols(c)],
            dst_ref=out_ref.at[core, me, :, cols(c)],
            send_sem=send_sem.at[d, c],
            recv_sem=recv_sem.at[d, c],
            device_id={"ep": dst},
            device_id_type=MESH,
        )

    def from_peer(d, c):
        src = lax.rem(me - d + n_ep, n_ep)
        return pltpu.make_async_remote_copy(
            src_ref=mine_ref.at[me, :, cols(c)],
            dst_ref=out_ref.at[core, src, :, cols(c)],
            send_sem=send_sem.at[d, c],
            recv_sem=recv_sem.at[d, c],
            device_id={"ep": src},
            device_id_type=MESH,
        )

    def forward(d, c, side):
        src = lax.rem(me - d + n_ep, n_ep)
        source = mine_ref.at[me, :, cols(c)] if d == 0 else out_ref.at[side, src, :, cols(c)]
        return pltpu.make_async_remote_copy(
            src_ref=source,
            dst_ref=out_ref.at[side, src, :, cols(c)],
            send_sem=fwd_send.at[d, c],
            recv_sem=fwd_recv.at[d, c],
            device_id={"tp": partner},
            device_id_type=MESH,
        )

    def swap(d, c, arriving):
        src = lax.rem(me - d + n_ep, n_ep)
        ref = out_ref.at[core, src, :, cols(c + DIRECT if arriving else c)]
        return pltpu.make_async_remote_copy(
            src_ref=ref,
            dst_ref=ref,
            send_sem=z_send.at[d, c],
            recv_sem=z_recv.at[d, c],
            device_id={"tp": across},
            device_id_type=MESH,
        )

    order = sorted(range(1, n_ep), key=lambda d: abs(d - n_ep // 2))
    extra = CHUNKS - DIRECT
    for c in range(DIRECT):
        for d in order:
            to_peer(d, c).start()
    keep = pltpu.make_async_copy(mine_ref.at[me], out_ref.at[core, me], local_sem)
    keep.start()
    for c in range(CHUNKS):
        forward(0, c, core).start()
    lag = DIRECT - extra
    for c in range(DIRECT):
        for d in order:
            from_peer(d, c).wait_recv()
            if c < extra:
                swap(d, c, False).start()
            forward(d, c, core).start()
        if c >= lag:
            for d in order:
                swap(d, c - lag, True).wait_recv()
                forward(d, c - lag + DIRECT, core).start()
    keep.wait()
    for c in range(DIRECT):
        for d in order:
            to_peer(d, c).wait_send()
    for c in range(extra):
        for d in order:
            swap(d, c, False).wait_send()
    for d in range(n_ep):
        for c in range(CHUNKS):
            forward(d, c, core).wait_send()
            forward(d, c, 1 - core).wait_recv()


def dispatch(mine, n_ep):
    return pl.pallas_call(
        functools.partial(dispatch_kernel, n_ep),
        out_shape=jax.ShapeDtypeStruct((2,) + mine.shape, mine.dtype),
        in_specs=[pl.BlockSpec(memory_space=pltpu.VMEM)],
        out_specs=pl.BlockSpec(memory_space=pl.ANY),
        scratch_shapes=[
            pltpu.SemaphoreType.DMA,
            pltpu.SemaphoreType.DMA((n_ep, CHUNKS)),
            pltpu.SemaphoreType.DMA((n_ep, CHUNKS)),
            pltpu.SemaphoreType.DMA((n_ep, CHUNKS)),
            pltpu.SemaphoreType.DMA((n_ep, CHUNKS)),
            pltpu.SemaphoreType.DMA((n_ep, CHUNKS)),
            pltpu.SemaphoreType.DMA((n_ep, CHUNKS)),
        ],
        compiler_params=pltpu.CompilerParams(collective_id=0, has_side_effects=True),
        name="dispatch",
    )(mine)


def sums_kernel(n_ep, n_tp, part_ref, norm_ref, score_ref, slots, total, send_sem, recv_sem, s_send, s_recv):
    me = lax.axis_index("ep")
    t = lax.axis_index("tp")
    barrier = pltpu.get_barrier_semaphore()
    for d in range(1, n_tp):
        pl.semaphore_signal(
            barrier, inc=1, device_id={"tp": lax.rem(t + d, n_tp)}, device_id_type=MESH
        )
    for d in range(1, n_ep):
        pl.semaphore_signal(
            barrier, inc=1, device_id={"ep": lax.rem(me + d, n_ep)}, device_id_type=MESH
        )
    pl.semaphore_wait(barrier, n_tp - 1 + n_ep - 1)

    def part_to(d):
        return pltpu.make_async_remote_copy(
            src_ref=part_ref,
            dst_ref=slots.at[t],
            send_sem=send_sem.at[d],
            recv_sem=recv_sem.at[d],
            device_id={"tp": lax.rem(t + d, n_tp)},
            device_id_type=MESH,
        )

    def part_from(d):
        src = lax.rem(t - d + n_tp, n_tp)
        return pltpu.make_async_remote_copy(
            src_ref=part_ref,
            dst_ref=slots.at[src],
            send_sem=send_sem.at[d],
            recv_sem=recv_sem.at[d],
            device_id={"tp": src},
            device_id_type=MESH,
        )

    for d in range(1, n_tp):
        part_to(d).start()
    slots[t] = part_ref[...]
    for d in range(1, n_tp):
        part_from(d).wait_recv()
    acc = slots[0]
    for i in range(1, n_tp):
        acc = acc + slots[i]
    total[...] = acc
    rows = 8 * n_ep

    def score_to(d):
        dst = lax.rem(me + d, n_ep)
        return pltpu.make_async_remote_copy(
            src_ref=total.at[pl.ds(pl.multiple_of(dst * 8, 8), 8)],
            dst_ref=score_ref.at[me],
            send_sem=s_send.at[d],
            recv_sem=s_recv.at[d],
            device_id={"ep": dst},
            device_id_type=MESH,
        )

    def score_from(d):
        src = lax.rem(me - d + n_ep, n_ep)
        return pltpu.make_async_remote_copy(
            src_ref=total.at[pl.ds(0, 8)],
            dst_ref=score_ref.at[src],
            send_sem=s_send.at[d],
            recv_sem=s_recv.at[d],
            device_id={"ep": src},
            device_id_type=MESH,
        )

    norm_ref[...] = acc[rows:]
    for d in range(1, n_tp):
        part_to(d).wait_send()
    for d in range(1, n_ep):
        score_to(d).start()
    score_ref[me] = total[pl.ds(pl.multiple_of(me * 8, 8), 8)]
    for d in range(1, n_ep):
        score_from(d).wait_recv()
    for d in range(1, n_ep):
        score_to(d).wait_send()


def small_sums(scores, norms, n_ep, n_tp):
    cap = scores.shape[1]
    width = norms.shape[1]
    padded = jnp.pad(scores, ((0, 0), (0, 1024 - cap))).reshape(n_ep * 8, 128)
    part = jnp.concatenate([padded, norms.reshape(2 * width // 128, 128)], axis=0)
    norm_out, score_out = pl.pallas_call(
        functools.partial(sums_kernel, n_ep, n_tp),
        out_shape=(
            jax.ShapeDtypeStruct((2 * width // 128, 128), jnp.float32),
            jax.ShapeDtypeStruct((n_ep, 8, 128), jnp.float32),
        ),
        in_specs=[pl.BlockSpec(memory_space=pltpu.VMEM)],
        out_specs=(
            pl.BlockSpec(memory_space=pltpu.VMEM),
            pl.BlockSpec(memory_space=pltpu.VMEM),
        ),
        scratch_shapes=[
            pltpu.VMEM((n_tp,) + part.shape, jnp.float32),
            pltpu.VMEM(part.shape, jnp.float32),
            pltpu.SemaphoreType.DMA((n_tp,)),
            pltpu.SemaphoreType.DMA((n_tp,)),
            pltpu.SemaphoreType.DMA((n_ep,)),
            pltpu.SemaphoreType.DMA((n_ep,)),
        ],
        compiler_params=pltpu.CompilerParams(collective_id=1, has_side_effects=True),
        cost_estimate=pl.CostEstimate(flops=0, bytes_accessed=20_000_000, transcendentals=0),
        name="small_sums",
    )(part)
    return score_out.reshape(n_ep, 1024)[:, :cap], norm_out.reshape(2, width)


def fused_kernel(
    n_ep, n_tp, cap, tok_ref, cot_ref, gate_ref, up_ref, down_ref, route_hbm, group_hbm, prob_hbm,
    token_out, gate_g, up_g, down_g, gate_norm, up_norm, down_norm, prob_grad, group_grad,
    route_ref, group_ref, prob_ref, src_v, gate_v, up_v, down_v, mine, rows, gate_p, up_p, hid_p, pick_v, pick_t,
    part_out, part_in, part_own, part_sum, returned,
    tok_f, tok_b, a_in, b_out, b_in,
    norm_part, norm_in, norm_z, norm_fin, score_part, score_in, score_z, score_tot, score_ep,
    load_sem, sx, rx, zs, zr, fs, fr, ps, pr, es, er, a_s, a_r, b_s, b_r, c_s, c_r, e_s, e_r, q_s, q_r,
    f_s, f_r, ns, nr, nzs, nzr, nfs, nfr, ss, sr, szs, szr, ses, ser,
):
    bf, f32 = jnp.bfloat16, jnp.float32
    me = lax.axis_index("ep")
    t = lax.axis_index("tp")
    core = lax.rem(t, 2)
    z = t // 2
    nz = n_tp // 2
    side = lax.rem(z, 2)
    partner = t + 1 - 2 * core
    across = t + 2 - 4 * side
    middle = jnp.logical_and(z > 0, z < nz - 1)
    end = jnp.logical_or(z == 0, z == nz - 1)
    tok, width = token_out.shape
    ff = gate_v.shape[1]
    half = width // 2
    mid_peer = lax.rem(t + 2 * (3 - 2 * z) + n_tp, n_tp)
    peers = {1: me + 1 - 2 * lax.rem(me, 2), 2: lax.rem(me + 2, n_ep), 3: n_ep - 1 - me}

    def remote(src, dst, send, recv, device):
        return pltpu.make_async_remote_copy(
            src_ref=src, dst_ref=dst, send_sem=send, recv_sem=recv,
            device_id=device, device_id_type=MESH,
        )

    @pl.when(core == 0)
    def _():
        pltpu.make_async_copy(tok_ref, src_v, load_sem.at[0]).start()

    @pl.when(core == 1)
    def _():
        pltpu.make_async_copy(cot_ref, src_v, load_sem.at[0]).start()

    small = [
        pltpu.make_async_copy(a, b, load_sem.at[n + 4])
        for n, (a, b) in enumerate(
            ((route_hbm, route_ref), (group_hbm, group_ref), (prob_hbm, prob_ref))
        )
    ]
    for copy in small:
        copy.start()
    loads = [
        pltpu.make_async_copy(a, b, load_sem.at[n + 1])
        for n, (a, b) in enumerate(((gate_ref, gate_v), (up_ref, up_v), (down_ref, down_v)))
    ]
    for copy in loads:
        copy.start()

    barrier = pltpu.get_barrier_semaphore()
    for d in range(1, n_ep):
        pl.semaphore_signal(barrier, inc=1, device_id={"ep": peers[d]}, device_id_type=MESH)
    for d in range(1, nz):
        pl.semaphore_signal(
            barrier, inc=1, device_id={"tp": lax.rem(t + 2 * d, n_tp)}, device_id_type=MESH
        )
    pl.semaphore_signal(barrier, inc=1, device_id={"tp": partner}, device_id_type=MESH)

    for copy in small:
        copy.wait()
    order = [1, 2, 3, 0]
    first, second = route_ref[0:1, :], route_ref[1:2, :]
    weight = group_ref[...] * prob_ref[...]
    w0, w1 = weight[0:1, :], weight[1:2, :]
    experts = [me if d == 0 else peers[d] for d in range(n_ep)]
    hit0 = [first == e for e in experts]
    hit1 = [second == e for e in experts]
    named = [jnp.where(jnp.logical_or(x, y), 1.0, 0.0) for x, y in zip(hit0, hit1)]
    weight_of = [jnp.where(x, w0, 0.0) + jnp.where(y, w1, 0.0) for x, y in zip(hit0, hit1)]
    named8 = jnp.concatenate(named + [jnp.zeros((8 - n_ep, tok), f32)], axis=0)
    earlier = jnp.where(
        lax.broadcasted_iota(jnp.int32, (tok, tok), 0) < lax.broadcasted_iota(jnp.int32, (tok, tok), 1),
        1.0, 0.0,
    ).astype(bf)
    before = jnp.dot(named8.astype(bf), earlier, preferred_element_type=f32)
    place = jnp.where(named8 > 0.5, before, -1.0)
    slot = lax.broadcasted_iota(jnp.int32, (cap, tok), 0).astype(f32)
    is_cot = core.astype(f32)
    with jax.named_scope("w_src"):
        pltpu.make_async_copy(tok_ref, src_v, load_sem.at[0]).wait()

    sizes = [cap // 6, cap // 6, cap // 3]
    starts = [0, cap // 6, cap // 3]

    def span(c, s):
        at = starts[c] + s * (cap - 2 * starts[c] - sizes[c])
        return pl.multiple_of(at, 16), sizes[c]

    def block_rows(d, c, s):
        at, n = span(c, s)
        return pl.ds(pl.multiple_of(d * cap + at, 16), n)

    def to_peer(d, c):
        at, n = span(c, side)
        return remote(
            mine.at[d - 1, pl.ds(at, n)], rows.at[core, block_rows(d, c, side)],
            sx.at[d, c], rx.at[d, c], {"ep": peers[d]},
        )

    def swap(d, c, arriving):
        at = block_rows(d, c, 1 - side if arriving else side)
        ref = rows.at[core, at]
        return remote(ref, ref, zs.at[d, c], zr.at[d, c], {"tp": across})

    def share(d, c, swapped, kind):
        if d == 0:
            at = pl.ds(0, cap)
        else:
            at = block_rows(d, c, 1 - side if swapped else side)
        ref = rows.at[kind, at]
        n = c + 3 * swapped
        return remote(ref, ref, fs.at[d, n], fr.at[d, n], {"tp": partner})

    pieces = [(d, c, s) for d in range(1, n_ep) for c, s in ((0, 0), (1, 0), (2, 0), (0, 1), (1, 1))]

    greeted = False
    for d in order:
        with jax.named_scope("mine"):
            pick = jnp.where(slot == place[d:d + 1, :], 1.0, 0.0)
            pick_v[d] = pick.astype(bf)
            slot_weight = jnp.sum(pick * weight_of[d], axis=1, keepdims=True)
            factor = slot_weight * is_cot + (1.0 - is_cot)
            for n in range(0, width, 512):
                got = jnp.dot(pick_v[d], src_v[:, n:n + 512], preferred_element_type=f32)
                got = (got * factor).astype(bf)
                if d == 0:
                    rows[core, 0:cap, n:n + 512] = got
                else:
                    mine[d - 1, :, n:n + 512] = got
            if not greeted:
                with jax.named_scope("barrier"):
                    pl.semaphore_wait(barrier, n_ep - 1 + nz)
                greeted = True
            if d == 0:
                share(0, 0, 0, core).start()
            elif d == 3:
                for e, c in ((3, 0), (1, 2), (2, 2), (3, 1), (3, 2)):
                    to_peer(e, c).start()
            else:
                for c in (0, 1):
                    to_peer(d, c).start()

    column = jnp.transpose(place)
    lane = lax.broadcasted_iota(jnp.int32, (tok, cap), 1).astype(f32)
    for d in range(n_ep):
        pick_t[d] = jnp.where(lane == column[:, d:d + 1], 1.0, 0.0).astype(bf)

    last = (((1,), (1,)), ((), ()))
    contract = (((0,), (0,)), ((), ()))

    def fold(sq):
        parts = [sq[:, j * 128:(j + 1) * 128] for j in range(sq.shape[1] // 128)]
        return functools.reduce(jnp.add, parts)

    mine_half = pl.multiple_of(core * half, 128)
    other_half = pl.multiple_of((1 - core) * half, 128)

    def exchange(lo, n):
        at = pl.ds(lo * cap, n * cap)
        return remote(part_out.at[at], part_in.at[at], ps.at[lo], pr.at[lo], {"tp": partner})

    jw = 128
    steps = half // jw
    groups = ((0, 1), (1, 2), (3, 1))

    def back(d, j):
        w = jw if d == 3 else half // 2
        at = pl.ds(j * w, w)
        return remote(
            part_sum.at[d - 1, :, at], returned.at[d, :, at], es.at[d, j], er.at[d, j], {"ep": peers[d]}
        )

    def block(lo, count, between=()):
        at = slice(lo * cap, (lo + count) * cap)
        score = None
        for n in range(0, ff, 256):
            with jax.named_scope("fwd"):
                pre_gate = jnp.dot(rows[0, at, :], gate_v[:, n:n + 256], preferred_element_type=f32)
                pre_up = jnp.dot(rows[0, at, :], up_v[:, n:n + 256], preferred_element_type=f32)
                grad = lax.dot_general(rows[1, at, :], down_v[n:n + 256, :], last, preferred_element_type=f32)
                sigma = jax.nn.sigmoid(pre_gate)
                activated = pre_gate * sigma
                derivative = sigma * (1.0 + pre_gate * (1.0 - sigma))
                hidden = (activated * pre_up).astype(bf)
                hid_p[at, n:n + 256] = hidden
                more = fold(hidden.astype(f32) * grad)
                score = more if score is None else score + more
                gate_p[at, n:n + 256] = (grad * pre_up * derivative).astype(bf)
                up_p[at, n:n + 256] = (grad * activated).astype(bf)
        for i in range(count):
            score_part[lo + i:lo + i + 1, 0:cap] = jnp.sum(
                jnp.transpose(score[i * cap:(i + 1) * cap]), axis=0, keepdims=True
            )

        def part(c):
            got = lax.dot_general(gate_p[at, :], gate_v[pl.ds(c, 256), :], last, preferred_element_type=f32)
            return got + lax.dot_general(
                up_p[at, :], up_v[pl.ds(c, 256), :], last, preferred_element_type=f32
            )

        with jax.named_scope("part_other"):
            for n in range(0, half, 256):
                part_out[at, n:n + 256] = part(pl.multiple_of(other_half + n, 128)).astype(bf)
        exchange(lo, count).start()
        for step in between:
            step()
        with jax.named_scope("part_own"):
            for n in range(0, half, 256):
                part_own[0:count * cap, n:n + 256] = part(pl.multiple_of(mine_half + n, 128))
        with jax.named_scope("w_part"):
            exchange(lo, count).wait_recv()
        for n in range(0, half, 256):
            total = part_own[0:count * cap, n:n + 256] + part_in[at, n:n + 256].astype(f32)
            total = total.astype(bf)
            for i in range(count):
                piece = total[i * cap:(i + 1) * cap]
                if lo == 0:
                    returned[0, :, n:n + 256] = piece
                else:
                    part_sum[lo + i - 1, :, n:n + 256] = piece
        if lo == 3:
            for j in range(steps // 2):
                back(3, j).start()
            back(1, 1).start()
            back(2, 1).start()
            for j in range(steps // 2, steps):
                back(3, j).start()
        elif lo:
            back(1, 0).start()
            back(2, 0).start()

    def arrive(d, c):
        to_peer(d, c).wait_recv()
        if c < 2:
            swap(d, c, False).start()
        share(d, c, 0, core).start()

    def arrive_swap(d, c):
        swap(d, c, True).wait_recv()
        share(d, c, 1, core).start()

    def shared(d):
        for c, s in ((0, 0), (1, 0), (2, 0), (0, 1), (1, 1)):
            share(d, c, s, 1 - core).wait_recv()

    score_part[...] = jnp.zeros_like(score_part)
    with jax.named_scope("w_own"):
        share(0, 0, 0, 1 - core).wait_recv()
        for copy in loads:
            copy.wait()
    block(0, 1, (lambda: arrive(1, 0), lambda: arrive(2, 0)))
    with jax.named_scope("w_1"):
        arrive(1, 1)
        arrive(2, 1)
    with jax.named_scope("w_g0"):
        arrive(3, 0)
    with jax.named_scope("w_swap0"):
        arrive_swap(1, 0)
        arrive_swap(2, 0)
    with jax.named_scope("w_2"):
        arrive(1, 2)
        arrive(2, 2)
    with jax.named_scope("w_swap1"):
        arrive_swap(1, 1)
        arrive_swap(2, 1)
    with jax.named_scope("w_sh12"):
        shared(1)
        shared(2)
    block(1, 2, (lambda: arrive(3, 1),))
    with jax.named_scope("w_gswap0"):
        arrive_swap(3, 0)
    with jax.named_scope("w_g2"):
        arrive(3, 2)
    with jax.named_scope("w_gswap1"):
        arrive_swap(3, 1)
    with jax.named_scope("w_gsh"):
        shared(3)
    block(3, 1)

    def score_pair():
        return remote(score_part, score_in, ss, sr, {"tp": partner})

    def score_to(d):
        return remote(score_tot, score_z.at[z], szs.at[d], szr.at[d], {"tp": lax.rem(t + 2 * d, n_tp)})

    def score_from(d):
        src = lax.rem(z - d + nz, nz)
        return remote(
            score_tot, score_z.at[src], szs.at[d], szr.at[d], {"tp": lax.rem(t - 2 * d + n_tp, n_tp)}
        )

    def score_back(d):
        return remote(score_fin, score_ep.at[d], ses.at[d], ser.at[d], {"ep": peers[d]})

    score_fin = score_in
    score_pair().start()

    def gate_up(k):
        at = pl.ds(pl.multiple_of(k * 256, 256), 256)
        lhs = rows[0, :, at]
        for n, (rhs, out) in enumerate(((gate_p, gate_g), (up_p, up_g))):
            total = lax.dot_general(lhs, rhs[...], contract, preferred_element_type=f32)
            out[at, :] = total.astype(bf)
            sq = fold(total * total)
            for h in range(2):
                norm_part[n, pl.ds(k * 2 + h, 1), :] = jnp.sum(
                    jnp.transpose(sq[h * 128:(h + 1) * 128]), axis=0, keepdims=True
                ) / (ff * n_tp)

    def loop_gate_up(lo, hi):
        def body(k, carry):
            gate_up(k)
            return carry
        lax.fori_loop(lo, hi, body, 0)

    def down(k):
        at = pl.ds(pl.multiple_of(k * 256, 256), 256)
        lhs = hid_p[:, at]
        sq = None
        for c in range(0, width, 512):
            total = lax.dot_general(lhs, rows[1, :, c:c + 512], contract, preferred_element_type=f32)
            down_g[at, c:c + 512] = total.astype(bf)
            more = fold(total * total)
            sq = more if sq is None else sq + more
        for h in range(2):
            down_norm[0:1, k * 256 + h * 128:k * 256 + (h + 1) * 128] = jnp.sum(
                jnp.transpose(sq[h * 128:(h + 1) * 128]), axis=0, keepdims=True
            ) / width

    def norm_pair():
        return remote(norm_part.at[1 - core], norm_in, ns, nr, {"tp": partner})

    def norm_to(d):
        return remote(norm_part.at[core], norm_z.at[z], nzs.at[d], nzr.at[d],
                      {"tp": lax.rem(t + 2 * d, n_tp)})

    def norm_from(d):
        src = lax.rem(z - d + nz, nz)
        return remote(norm_part.at[core], norm_z.at[src], nzs.at[d], nzr.at[d],
                      {"tp": lax.rem(t - 2 * d + n_tp, n_tp)})

    def norm_done(kind):
        ref = norm_fin.at[kind]
        return remote(ref, ref, nfs, nfr, {"tp": partner})

    def work_score_a():
        score_pair().wait_recv()
        score_pair().wait_send()
        score_tot[...] = score_part[...] + score_in[...]
        for d in range(1, nz):
            score_to(d).start()
        score_z[z] = score_tot[...]

    def work_norm_a():
        norm_pair().start()

    def work_norm_b():
        norm_pair().wait_recv()
        norm_pair().wait_send()
        norm_part[core] = norm_part[core] + norm_in[...]
        for d in range(1, nz):
            norm_to(d).start()
        norm_z[z] = norm_part[core]

    def work_score_b():
        for d in range(1, nz):
            score_from(d).wait_recv()
        score_fin[...] = functools.reduce(jnp.add, [score_z[i] for i in range(nz)])
        for d in range(1, n_ep):
            score_back(d).start()

    def work_norm_c():
        for d in range(1, nz):
            norm_from(d).wait_recv()
        norm_fin[core] = functools.reduce(jnp.add, [norm_z[i] for i in range(nz)])
        norm_done(core).start()

    def work_score_c():
        of0 = jnp.zeros((1, tok), f32)
        of1 = jnp.zeros((1, tok), f32)
        for d in range(n_ep):
            if d:
                score_back(d).wait_recv()
            line = score_fin if d == 0 else score_ep.at[d]
            hit = jnp.dot(
                line[:, 0:cap], pick_v[d].astype(f32), preferred_element_type=f32,
                precision=lax.Precision.HIGHEST,
            )
            hit = hit[d:d + 1, :]
            of0 = of0 + jnp.where(hit0[d], hit, 0.0)
            of1 = of1 + jnp.where(hit1[d], hit, 0.0)
        slot0, slot1 = of0 / w0, of1 / w1
        prob_grad[0:1, :] = group_ref[...] * slot0
        prob_grad[1:2, :] = group_ref[...] * slot1
        group_grad[...] = prob_ref[0:1, :] * slot0 + prob_ref[1:2, :] * slot1

    def work_norm_d():
        norm_done(1 - core).wait_recv()
        for i in range(width // 128):
            gate_norm[0:1, i * 128:(i + 1) * 128] = norm_fin[0, i:i + 1, :]
            up_norm[0:1, i * 128:(i + 1) * 128] = norm_fin[1, i:i + 1, :]

    strips = width // 256
    with jax.named_scope("gate_up"):
        loop_gate_up(0, strips // 2)
    with jax.named_scope("score_a"):
        work_score_a()

    th = tok // 2
    own_at = pl.multiple_of((z - 1) * th, 128)
    far_at = pl.multiple_of((2 - z) * th, 128)

    def cols(c, j):
        return pl.ds(pl.multiple_of(c * half + j * jw, 128), jw)

    def a_copy(j):
        return remote(tok_b.at[j], a_in.at[j], a_s.at[j], a_r.at[j], {"tp": across})

    def b_copy(j):
        return remote(b_out.at[j], b_in.at[j], b_s.at[j], b_r.at[j], {"tp": mid_peer})

    def c_copy(j, at):
        ref = token_out.at[pl.ds(at, th), cols(core, j)]
        return remote(ref, ref, c_s.at[j], c_r.at[j], {"tp": mid_peer})

    def e_copy(j, at):
        ref = token_out.at[pl.ds(at, th), cols(core, j)]
        return remote(ref, ref, e_s.at[j], e_r.at[j], {"tp": across})

    def q_copy(j, at):
        ref = token_out.at[pl.ds(at, th), cols(core, j)]
        return remote(ref, ref, q_s.at[j], q_r.at[j], {"tp": across})

    def f_copy(j, c):
        ref = token_out.at[:, cols(c, j)]
        return remote(ref, ref, f_s.at[j], f_r.at[j], {"tp": partner})

    near_at = pl.multiple_of(jnp.where(z == 0, 0, th), 128)
    beyond_at = pl.multiple_of(jnp.where(z == 0, th, 0), 128)

    lag_a, lag_b, lag_c, lag_e = 1, 3, 5, steps

    def combine(j):
        if j % (steps // 2) == 0:
            back(1, 2 * j // steps).wait_recv()
            back(2, 2 * j // steps).wait_recv()
        back(3, j).wait_recv()
        at = slice(j * jw, (j + 1) * jw)
        total = None
        for d in range(n_ep):
            more = jnp.dot(pick_t[d], returned[d, :, at], preferred_element_type=f32)
            total = more if total is None else total + more

        @pl.when(end)
        def _():
            tok_b[j] = total.astype(bf)
            a_copy(j).start()

        @pl.when(middle)
        def _():
            tok_f[j] = total

    def pair_sum(j):
        @pl.when(middle)
        def _():
            a_copy(j).wait_recv()
            b_out[j] = (
                tok_f[j, pl.ds(far_at, th), :] + a_in[j, pl.ds(far_at, th), :].astype(f32)
            ).astype(bf)
            b_copy(j).start()
            tok_f[j, pl.ds(own_at, th), :] = (
                tok_f[j, pl.ds(own_at, th), :] + a_in[j, pl.ds(own_at, th), :].astype(f32)
            )

    def line_sum(j):
        @pl.when(middle)
        def _():
            b_copy(j).wait_recv()
            token_out[pl.ds(own_at, th), cols(core, j)] = (
                tok_f[j, pl.ds(own_at, th), :] + b_in[j].astype(f32)
            ).astype(bf)
            c_copy(j, own_at).start()
            e_copy(j, own_at).start()

    def relay(j):
        @pl.when(middle)
        def _():
            c_copy(j, far_at).wait_recv()
            q_copy(j, far_at).start()
            f_copy(j, core).start()

    def collect(j):
        @pl.when(end)
        def _():
            e_copy(j, near_at).wait_recv()
            q_copy(j, beyond_at).wait_recv()
            f_copy(j, core).start()

    left = strips - strips // 2
    filler = {
        i: [lambda i=i: loop_gate_up(strips // 2 + i * left // 3, strips // 2 + (i + 1) * left // 3)]
        for i in range(3)
    }
    filler[1].append(work_score_b)
    filler[3] = [work_norm_a, lambda: down(0)]
    filler[4] = [work_norm_b]
    filler[5] = [lambda: down(1)]
    stages = (
        ("combine", 0, combine), ("pair_sum", lag_a, pair_sum), ("line_sum", lag_b, line_sum),
        ("relay", lag_c, relay), ("collect", lag_e, collect),
    )
    for s in range(steps + lag_e):
        for name, lag, step in stages:
            if 0 <= s - lag < steps:
                with jax.named_scope(name):
                    step(s - lag)
        for item in filler.get(s, []):
            with jax.named_scope("filler"):
                item()

    with jax.named_scope("last"):
        work_score_c()
        work_norm_c()
        work_norm_d()

    with jax.named_scope("w_final"):
        for j in range(steps):
            f_copy(j, 1 - core).wait_recv()
            f_copy(j, core).wait_send()
            back(3, j).wait_send()

    @pl.when(end)
    def _():
        for j in range(steps):
            a_copy(j).wait_send()

    @pl.when(middle)
    def _():
        for j in range(steps):
            b_copy(j).wait_send()
            c_copy(j, own_at).wait_send()
            e_copy(j, own_at).wait_send()
            q_copy(j, far_at).wait_send()

    for lo, n in groups:
        exchange(lo, n).wait_send()
    for d in (1, 2):
        back(d, 0).wait_send()
        back(d, 1).wait_send()
    share(0, 0, 0, core).wait_send()
    for d, c, s in pieces:
        share(d, c, s, core).wait_send()
        if not s:
            to_peer(d, c).wait_send()
            if c < 2:
                swap(d, c, False).wait_send()
    for d in range(1, nz):
        score_to(d).wait_send()
        norm_to(d).wait_send()
    for d in range(1, n_ep):
        score_back(d).wait_send()
    norm_done(core).wait_send()


def store_kernel(count, *refs):
    sem = refs[-1]
    copies = [pltpu.make_async_copy(refs[n], refs[count + n], sem.at[n]) for n in range(count)]
    for copy in copies:
        copy.start()
    for copy in copies:
        copy.wait()


def fused(tokens, cotangent, group_prob, expert_prob, routing, gate_weight, up_weight, down_weight):
    tok, width = tokens.shape
    n_ep = lax.axis_size("ep")
    n_tp = lax.axis_size("tp")
    ff = gate_weight.shape[2]
    cap = 3 * tok * routing.shape[1] // (2 * n_ep)
    slots = n_ep * cap
    nz = n_tp // 2
    half = width // 2
    jw = 128
    steps = half // jw
    th = tok // 2
    bf, f32 = jnp.bfloat16, jnp.float32
    vm = pltpu.VMEM
    dma = pltpu.SemaphoreType.DMA
    vmem = pl.BlockSpec(memory_space=pltpu.VMEM)
    hbm = pl.BlockSpec(memory_space=pl.ANY)
    shapes = (
        jax.ShapeDtypeStruct((tok, width), bf),
        jax.ShapeDtypeStruct((width, ff), bf),
        jax.ShapeDtypeStruct((width, ff), bf),
        jax.ShapeDtypeStruct((ff, width), bf),
        jax.ShapeDtypeStruct((1, width), f32),
        jax.ShapeDtypeStruct((1, width), f32),
        jax.ShapeDtypeStruct((1, ff), f32),
        jax.ShapeDtypeStruct((2, tok), f32),
        jax.ShapeDtypeStruct((1, tok), f32),
    )
    count = len(shapes)
    outs = pl.pallas_call(
        functools.partial(fused_kernel, n_ep, n_tp, cap),
        out_shape=tuple(pltpu.VMEM(x.shape, x.dtype) for x in shapes),
        in_specs=[hbm] * 8,
        out_specs=(vmem,) * count,
        scratch_shapes=[
            vm((2, tok), jnp.int32), vm((1, tok), f32), vm((2, tok), f32),
            vm((tok, width), bf), vm((width, ff), bf), vm((width, ff), bf), vm((ff, width), bf),
            vm((n_ep - 1, cap, width), bf), vm((2, slots, width), bf),
            vm((slots, ff), bf), vm((slots, ff), bf), vm((slots, ff), bf),
            vm((n_ep, cap, tok), bf), vm((n_ep, tok, cap), bf),
            vm((slots, half), bf), vm((slots, half), bf), vm((2 * cap, half), f32),
            vm((n_ep - 1, cap, half), bf), vm((n_ep, cap, half), bf),
            vm((steps, tok, jw), f32), vm((steps, tok, jw), bf), vm((steps, tok, jw), bf),
            vm((steps, th, jw), bf), vm((steps, th, jw), bf),
            vm((2, width // 128, 128), f32), vm((width // 128, 128), f32),
            vm((nz, width // 128, 128), f32), vm((2, width // 128, 128), f32),
            vm((8, tok), f32), vm((8, tok), f32), vm((nz, 8, tok), f32), vm((8, tok), f32),
            vm((n_ep, 8, tok), f32),
            dma((7,)), dma((n_ep, 3)), dma((n_ep, 3)), dma((n_ep, 2)), dma((n_ep, 2)),
            dma((n_ep, 5)), dma((n_ep, 5)), dma((n_ep,)), dma((n_ep,)),
            dma((n_ep, steps)), dma((n_ep, steps)),
        ] + [dma((steps,))] * 12 + [
            dma, dma, dma((nz,)), dma((nz,)), dma, dma, dma, dma, dma((nz,)), dma((nz,)),
            dma((n_ep,)), dma((n_ep,)),
        ],
        compiler_params=pltpu.CompilerParams(
            collective_id=3, has_side_effects=True, vmem_limit_bytes=56 << 20
        ),
        name="fused",
    )(
        tokens, cotangent, gate_weight[0], up_weight[0], down_weight[0],
        routing.T, group_prob.reshape(1, tok), expert_prob.T,
    )
    outs = pl.pallas_call(
        functools.partial(store_kernel, count),
        out_shape=shapes,
        in_specs=[vmem] * count,
        out_specs=(hbm,) * count,
        scratch_shapes=[dma((count,))],
        compiler_params=pltpu.CompilerParams(vmem_limit_bytes=1 << 20),
        name="store",
    )(*outs)
    token_grad, gate_g, up_g, down_g, gate_n, up_n, down_n, prob_g, group_g = outs
    return (
        token_grad, group_g.reshape(tok), prob_g.T, gate_g[None], up_g[None], down_g[None],
        gate_n, up_n, down_n,
    )


def general(tokens, cotangent, group_prob, expert_prob, routing, gate_weight, up_weight, down_weight):
    tok_count, model_width = tokens.shape
    top_count = routing.shape[1]
    n_ep = lax.axis_size("ep")
    n_tp = lax.axis_size("tp")
    capacity = 3 * tok_count * top_count // (2 * n_ep)
    buffer_rows = n_ep * capacity
    core = lax.rem(lax.axis_index("tp"), 2)
    weight = group_prob[:, None] * expert_prob

    experts = jnp.arange(n_ep, dtype=jnp.int32)[:, None]
    picks = [routing[None, :, k] == experts for k in range(top_count)]
    named = functools.reduce(jnp.logical_or, picks)
    weight_of = sum(jnp.where(picks[k], weight[None, :, k], 0.0) for k in range(top_count))
    earlier = (
        lax.broadcasted_iota(jnp.int32, (tok_count, tok_count), 0)
        < lax.broadcasted_iota(jnp.int32, (tok_count, tok_count), 1)
    ).astype(jnp.bfloat16)
    before = jnp.dot(named.astype(jnp.bfloat16), earlier, preferred_element_type=jnp.float32)
    place = jnp.where(named, before.astype(jnp.int32), -1)
    filled = place[:, None, :] == lax.broadcasted_iota(jnp.int32, (n_ep, capacity, tok_count), 1)
    pick = filled.astype(jnp.bfloat16).reshape(buffer_rows, tok_count)
    slot_weight = jnp.sum(jnp.where(filled, weight_of[:, None, :], 0.0), axis=2).reshape(buffer_rows, 1)

    source = jnp.where(core == 0, tokens, cotangent)
    factor = jnp.where(core == 0, 1.0, slot_weight)
    mine = jnp.dot(pick, source, preferred_element_type=jnp.float32) * factor
    mine = mine.astype(jnp.bfloat16).reshape(n_ep, capacity, model_width)
    both = dispatch(mine, n_ep)
    flat_in = both[0].reshape(buffer_rows, model_width)
    flat_scaled = both[1].reshape(buffer_rows, model_width)

    w_gate = gate_weight[0]
    w_up = up_weight[0]
    w_down = down_weight[0]
    hidden_total = gate_weight.shape[2] * n_tp
    contract_last = (((1,), (1,)), ((), ()))
    contract_rows = (((0,), (0,)), ((), ()))
    pre_gate = jnp.dot(flat_in, w_gate, preferred_element_type=jnp.float32)
    pre_up = jnp.dot(flat_in, w_up, preferred_element_type=jnp.float32)
    sigma = jax.nn.sigmoid(pre_gate)
    activated = pre_gate * sigma
    derivative = sigma * (1.0 + pre_gate * (1.0 - sigma))
    hidden = (activated * pre_up).astype(jnp.bfloat16)
    hidden_grad = lax.dot_general(
        flat_scaled, w_down, contract_last, preferred_element_type=jnp.float32
    )
    score_part = jnp.sum(hidden.astype(jnp.float32) * hidden_grad, axis=1).reshape(n_ep, capacity)
    gate_pre = (hidden_grad * pre_up * derivative).astype(jnp.bfloat16)
    up_pre = (hidden_grad * activated).astype(jnp.bfloat16)
    input_part = lax.dot_general(
        gate_pre, w_gate, contract_last, preferred_element_type=jnp.float32
    )
    input_part = input_part + lax.dot_general(
        up_pre, w_up, contract_last, preferred_element_type=jnp.float32
    )
    input_part = input_part.astype(jnp.bfloat16).reshape(n_ep, capacity, model_width)
    share = lax.psum_scatter(input_part, "tp", scatter_dimension=2, tiled=True)

    down_sum = lax.dot_general(
        hidden, flat_scaled, contract_rows, preferred_element_type=jnp.float32
    )
    gate_sum = lax.dot_general(flat_in, gate_pre, contract_rows, preferred_element_type=jnp.float32)
    up_sum = lax.dot_general(flat_in, up_pre, contract_rows, preferred_element_type=jnp.float32)
    norm_part = (
        jnp.stack([jnp.sum(gate_sum * gate_sum, axis=1), jnp.sum(up_sum * up_sum, axis=1)])
        / hidden_total
    )
    down_norms = jnp.sum(down_sum * down_sum, axis=1) / model_width
    scores, row_norms = small_sums(score_part, norm_part, n_ep, n_tp)

    share, scores, row_norms, down_norms = lax.optimization_barrier(
        (share, scores, row_norms, down_norms)
    )
    returned = lax.all_to_all(share, "ep", split_axis=0, concat_axis=0, tiled=True)
    returned = returned.reshape(buffer_rows, -1)
    token_share = lax.dot_general(pick, returned, contract_rows, preferred_element_type=jnp.float32)
    token_grad = lax.all_gather(token_share.astype(jnp.bfloat16), "tp", axis=1, tiled=True)
    gate_grad, up_grad, down_grad = (
        x.astype(jnp.bfloat16) for x in (gate_sum, up_sum, down_sum)
    )


    score_of = jnp.sum(jnp.where(filled, scores[:, :, None], 0.0), axis=1)
    slot_score = jnp.stack(
        [jnp.sum(jnp.where(p, score_of, 0.0), axis=0) for p in picks], axis=1
    ) / weight
    expert_prob_grad = group_prob[:, None] * slot_score
    group_prob_grad = jnp.sum(expert_prob * slot_score, axis=1)
    return (
        token_grad,
        group_prob_grad,
        expert_prob_grad,
        gate_grad[None],
        up_grad[None],
        down_grad[None],
        row_norms[0][None],
        row_norms[1][None],
        down_norms[None],
    )


def local(*args):
    n_ep, n_tp = lax.axis_size("ep"), lax.axis_size("tp")
    tok, width = args[0].shape
    ff = args[5].shape[2]
    cap = 3 * tok * args[4].shape[1] // (2 * n_ep)
    fits = cap % 96 == 0 and tok % 256 == 0 and width % 2048 == 0 and ff % 256 == 0
    if n_ep == 4 and n_tp == 8 and args[4].shape[1] == 2 and fits:
        return fused(*args)
    return general(*args)


def solution(mesh):
    return jax.shard_map(
        local,
        mesh=mesh,
        in_specs=(
            P("ep", None),
            P("ep", None),
            P("ep"),
            P("ep", None),
            P("ep", None),
            P("ep", None, "tp"),
            P("ep", None, "tp"),
            P("ep", "tp", None),
        ),
        out_specs=(
            P("ep", None),
            P("ep"),
            P("ep", None),
            P("ep", None, "tp"),
            P("ep", None, "tp"),
            P("ep", "tp", None),
            P("ep", None),
            P("ep", None),
            P("ep", "tp"),
        ),
        check_vma=False,
    )
```

time: 127 us -> 81.4 us (0.64)
  matrix products: 16.6 us -> 0 us
  local copies, waits for them, and re-layouts: 13.9 us -> 0 us
  Pallas kernels: 91.6 us -> 80.4 us
  other arithmetic: 3.74 us -> 0 us
    dot_general x7 -> x0, matrix products: 16.6 us -> none  [the longest x1 3.99 us: local(): mine = jnp.dot(pick, source, preferred_element_type=jnp.float32) * factor]
    pallas_call x2, Pallas kernels: 91.6 us -> 80.4 us  [the longest x1 77.3 us: fused(): pl.pallas_call(functools.partial(fused_kernel, n_ep, n_tp, cap), out_shap...]
    unnamed x26 -> x0, local copies, waits for them, and re-layouts: 7.61 us -> none
    slice x5 -> x0, local copies, waits for them, and re-layouts: 4.8 us -> none  [the longest x1 3.43 us: local(): flat_scaled = both[1].reshape(buffer_rows, model_width)]
    mul x2 -> x0, other arithmetic: 1.44 us -> none  [the longest x1 0.85 us: local(): weight = group_prob[:, None] * expert_prob]
    transpose x1 -> x0, other arithmetic: 1.28 us -> none  [local(): pick_t = pick.T]
where the time goes in v1:
time: 81.4 us; the launch traced here: 81.3 us
  Pallas kernels  80.4 us (99%)
    pallas_call x1, Pallas kernels, fused(): pl.pallas_call(functools.partial(fused_kernel, n_ep, n_tp, cap), out_shap...  77.3 us
    pallas_call x1, Pallas kernels, fused(): pl.pallas_call(functools.partial(store_kernel, count), out_shape=shapes,...  3.14 us

profile of v1, /device:TPU:0, one launch (start us, length us, event | category | flops | bytes accessed | tf_op | source)
XLA Modules:
  0.0 81.3 jit_solution(16140552698131919443)
XLA Ops:
  0.6 77.3 %fused.1 = (bf16[256,2048]{1,0:T(8,128)(2,1)S(1)}, bf16[2048,512]{1,0:T(8,128)(2,1)S(1)}, bf16[2048,512]{1,0:T(8,128)(2,1)S(1)}, bf16[512,2048]{1,0:T(8,128)(2,1...) custom-call(bf16[256,2048]{1,0:T(8,128)(2,1)} %tok_ref.1, ...), custom_call_target="tpu_custom_call" | custom-call | tf_op jit(solution)/shard_map/fused/pallas_call | solution.py:855
  78.0 3.1 %store.1 = (bf16[256,2048]{1,0:T(8,128)(2,1)}, bf16[2048,512]{1,0:T(8,128)(2,1)}, bf16[2048,512]{1,0:T(8,128)(2,1)}, bf16[512,2048]{1,0:T(8,128)(2,1)}, f32[1,20...) custom-call(bf16[256,2048]{1,0:T(8,128)(2,1)S(1)} %get-tuple-element.27.refs_0_, ...), custom_call_target="tpu_custom_call" | custom-call | tf_op jit(solution)/shard_map/store/pallas_call | solution.py:889

commit v2 on v1

--- a/solution.py
+++ b/solution.py
@@ -251,7 +251,7 @@
     tok_f, tok_b, a_in, b_out, b_in,
     norm_part, norm_in, norm_z, norm_fin, score_part, score_in, score_z, score_tot, score_ep,
     load_sem, sx, rx, zs, zr, fs, fr, ps, pr, es, er, a_s, a_r, b_s, b_r, c_s, c_r, e_s, e_r, q_s, q_r,
-    f_s, f_r, ns, nr, nzs, nzr, nfs, nfr, ss, sr, szs, szr, ses, ser,
+    g_s, g_r, f_s, f_r, ns, nr, nzs, nzr, nfs, nfr, ss, sr, szs, szr, ses, ser,
 ):
     bf, f32 = jnp.bfloat16, jnp.float32
     me = lax.axis_index("ep")
@@ -310,7 +310,8 @@
 
     for copy in small:
         copy.wait()
-    order = [1, 2, 3, 0]
+    order = [3, 1, 2, 0]
+    sends = {3: ((3, 0), (3, 1)), 1: ((1, 0), (1, 1)), 2: ((2, 0), (2, 1), (3, 2), (1, 2), (2, 2))}
     first, second = route_ref[0:1, :], route_ref[1:2, :]
     weight = group_ref[...] * prob_ref[...]
     w0, w1 = weight[0:1, :], weight[1:2, :]
@@ -331,8 +332,8 @@
     with jax.named_scope("w_src"):
         pltpu.make_async_copy(tok_ref, src_v, load_sem.at[0]).wait()
 
-    sizes = [cap // 6, cap // 6, cap // 3]
-    starts = [0, cap // 6, cap // 3]
+    sizes = [cap // 12, cap // 4, cap // 3]
+    starts = [0, cap // 12, cap // 3]
 
     def span(c, s):
         at = starts[c] + s * (cap - 2 * starts[c] - sizes[c])
@@ -385,12 +386,9 @@
                 greeted = True
             if d == 0:
                 share(0, 0, 0, core).start()
-            elif d == 3:
-                for e, c in ((3, 0), (1, 2), (2, 2), (3, 1), (3, 2)):
+            else:
+                for e, c in sends[d]:
                     to_peer(e, c).start()
-            else:
-                for c in (0, 1):
-                    to_peer(d, c).start()
 
     column = jnp.transpose(place)
     lane = lax.broadcasted_iota(jnp.int32, (tok, cap), 1).astype(f32)
@@ -407,20 +405,31 @@
     mine_half = pl.multiple_of(core * half, 128)
     other_half = pl.multiple_of((1 - core) * half, 128)
 
-    def exchange(lo, n):
-        at = pl.ds(lo * cap, n * cap)
-        return remote(part_out.at[at], part_in.at[at], ps.at[lo], pr.at[lo], {"tp": partner})
+    quarter = half // 2
+
+    def exchange(lo, n, h):
+        at = pl.ds(lo * cap, n * cap), pl.ds(h * quarter, quarter)
+        return remote(
+            part_out.at[at], part_in.at[at], ps.at[2 * lo + h], pr.at[2 * lo + h], {"tp": partner}
+        )
 
     jw = 128
     steps = half // jw
     groups = ((0, 1), (1, 2), (3, 1))
 
     def back(d, j):
-        w = jw if d == 3 else half // 2
+        w = jw if d == 3 else 2 * jw
         at = pl.ds(j * w, w)
         return remote(
             part_sum.at[d - 1, :, at], returned.at[d, :, at], es.at[d, j], er.at[d, j], {"ep": peers[d]}
         )
+
+    replies = {
+        (3, 0): [(3, j) for j in range(steps // 2)],
+        (3, 1): [(3, j) for j in range(steps // 2, steps - 2)],
+        (1, 0): [(1, 0), (2, 0), (3, steps - 2), (1, 1), (2, 1), (3, steps - 1)],
+        (1, 1): [(d, q) for q in range(2, steps // 2) for d in (1, 2)],
+    }
 
     def block(lo, count, between=()):
         at = slice(lo * cap, (lo + count) * cap)
@@ -450,36 +459,31 @@
                 up_p[at, :], up_v[pl.ds(c, 256), :], last, preferred_element_type=f32
             )
 
-        with jax.named_scope("part_other"):
-            for n in range(0, half, 256):
-                part_out[at, n:n + 256] = part(pl.multiple_of(other_half + n, 128)).astype(bf)
-        exchange(lo, count).start()
         for step in between:
-            step()
-        with jax.named_scope("part_own"):
-            for n in range(0, half, 256):
-                part_own[0:count * cap, n:n + 256] = part(pl.multiple_of(mine_half + n, 128))
-        with jax.named_scope("w_part"):
-            exchange(lo, count).wait_recv()
-        for n in range(0, half, 256):
-            total = part_own[0:count * cap, n:n + 256] + part_in[at, n:n + 256].astype(f32)
-            total = total.astype(bf)
-            for i in range(count):
-                piece = total[i * cap:(i + 1) * cap]
-                if lo == 0:
-                    returned[0, :, n:n + 256] = piece
-                else:
-                    part_sum[lo + i - 1, :, n:n + 256] = piece
-        if lo == 3:
-            for j in range(steps // 2):
-                back(3, j).start()
-            back(1, 1).start()
-            back(2, 1).start()
-            for j in range(steps // 2, steps):
-                back(3, j).start()
-        elif lo:
-            back(1, 0).start()
-            back(2, 0).start()
+            with jax.named_scope("between"):
+                step()
+        for h in (0, 1):
+            with jax.named_scope("part_other"):
+                for n in range(h * quarter, (h + 1) * quarter, 256):
+                    part_out[at, n:n + 256] = part(pl.multiple_of(other_half + n, 128)).astype(bf)
+            exchange(lo, count, h).start()
+        for h in (0, 1):
+            with jax.named_scope("part_own"):
+                for n in range(h * quarter, (h + 1) * quarter, 256):
+                    part_own[0:count * cap, n:n + 256] = part(pl.multiple_of(mine_half + n, 128))
+            with jax.named_scope("w_part"):
+                exchange(lo, count, h).wait_recv()
+            for n in range(h * quarter, (h + 1) * quarter, 256):
+                total = part_own[0:count * cap, n:n + 256] + part_in[at, n:n + 256].astype(f32)
+                total = total.astype(bf)
+                for i in range(count):
+                    piece = total[i * cap:(i + 1) * cap]
+                    if lo == 0:
+                        returned[0, :, n:n + 256] = piece
+                    else:
+                        part_sum[lo + i - 1, :, n:n + 256] = piece
+            for d, n in replies.get((lo, h), ()):
+                back(d, n).start()
 
     def arrive(d, c):
         to_peer(d, c).wait_recv()
@@ -500,34 +504,34 @@
         share(0, 0, 0, 1 - core).wait_recv()
         for copy in loads:
             copy.wait()
-    block(0, 1, (lambda: arrive(1, 0), lambda: arrive(2, 0)))
+    block(0, 1, (lambda: arrive(3, 0),))
     with jax.named_scope("w_1"):
+        arrive(3, 1)
+    with jax.named_scope("w_2"):
+        arrive(1, 0)
+        arrive(2, 0)
+    with jax.named_scope("w_swap0"):
+        arrive_swap(3, 0)
         arrive(1, 1)
         arrive(2, 1)
-    with jax.named_scope("w_g0"):
-        arrive(3, 0)
-    with jax.named_scope("w_swap0"):
+    with jax.named_scope("w_swap1"):
+        arrive_swap(3, 1)
         arrive_swap(1, 0)
         arrive_swap(2, 0)
-    with jax.named_scope("w_2"):
+    with jax.named_scope("w_g2"):
+        arrive(3, 2)
+    with jax.named_scope("w_gsh"):
+        shared(3)
+    block(3, 1, (lambda: arrive_swap(1, 1),))
+    with jax.named_scope("w_xy2"):
         arrive(1, 2)
         arrive(2, 2)
-    with jax.named_scope("w_swap1"):
-        arrive_swap(1, 1)
+    with jax.named_scope("w_xyswap"):
         arrive_swap(2, 1)
     with jax.named_scope("w_sh12"):
         shared(1)
         shared(2)
-    block(1, 2, (lambda: arrive(3, 1),))
-    with jax.named_scope("w_gswap0"):
-        arrive_swap(3, 0)
-    with jax.named_scope("w_g2"):
-        arrive(3, 2)
-    with jax.named_scope("w_gswap1"):
-        arrive_swap(3, 1)
-    with jax.named_scope("w_gsh"):
-        shared(3)
-    block(3, 1)
+    block(1, 2)
 
     def score_pair():
         return remote(score_part, score_in, ss, sr, {"tp": partner})
@@ -634,11 +638,13 @@
             if d:
                 score_back(d).wait_recv()
             line = score_fin if d == 0 else score_ep.at[d]
-            hit = jnp.dot(
-                line[:, 0:cap], pick_v[d].astype(f32), preferred_element_type=f32,
-                precision=lax.Precision.HIGHEST,
-            )
-            hit = hit[d:d + 1, :]
+            value = line[d:d + 1, 0:cap]
+            top = value.astype(bf).astype(f32)
+            rest = value - top
+            mid = rest.astype(bf).astype(f32)
+            parts = jnp.concatenate([top, mid, rest - mid, jnp.zeros((5, cap), f32)], axis=0)
+            hit = jnp.dot(parts.astype(bf), pick_v[d], preferred_element_type=f32)
+            hit = hit[0:1, :] + hit[1:2, :] + hit[2:3, :]
             of0 = of0 + jnp.where(hit0[d], hit, 0.0)
             of1 = of1 + jnp.where(hit1[d], hit, 0.0)
         slot0, slot1 = of0 / w0, of1 / w1
@@ -665,6 +671,19 @@
     def cols(c, j):
         return pl.ds(pl.multiple_of(c * half + j * jw, 128), jw)
 
+    far_end = lax.rem(t + n_tp // 2, n_tp)
+    direct, far = 1, 3
+    near_at = pl.multiple_of(jnp.where(z == 0, 0, th), 128)
+    beyond_at = pl.multiple_of(jnp.where(z == 0, th, 0), 128)
+
+    def near_copy(j):
+        return remote(tok_b.at[j, pl.ds(near_at, th)], a_in.at[j, pl.ds(0, th)], a_s.at[j], a_r.at[j],
+                      {"tp": across})
+
+    def beyond_copy(j):
+        return remote(tok_b.at[j, pl.ds(beyond_at, th)], a_in.at[j, pl.ds(th, th)], g_s.at[j], g_r.at[j],
+                      {"tp": far_end})
+
     def a_copy(j):
         return remote(tok_b.at[j], a_in.at[j], a_s.at[j], a_r.at[j], {"tp": across})
 
@@ -687,15 +706,17 @@
         ref = token_out.at[:, cols(c, j)]
         return remote(ref, ref, f_s.at[j], f_r.at[j], {"tp": partner})
 
-    near_at = pl.multiple_of(jnp.where(z == 0, 0, th), 128)
-    beyond_at = pl.multiple_of(jnp.where(z == 0, th, 0), 128)
+
+    def far_copy(j, at):
+        ref = token_out.at[pl.ds(at, th), cols(core, j)]
+        return remote(ref, ref, q_s.at[j], q_r.at[j], {"tp": far_end})
 
     lag_a, lag_b, lag_c, lag_e = 1, 3, 5, steps
 
     def combine(j):
-        if j % (steps // 2) == 0:
-            back(1, 2 * j // steps).wait_recv()
-            back(2, 2 * j // steps).wait_recv()
+        if j % 2 == 0:
+            back(1, j // 2).wait_recv()
+            back(2, j // 2).wait_recv()
         back(3, j).wait_recv()
         at = slice(j * jw, (j + 1) * jw)
         total = None
@@ -706,13 +727,23 @@
         @pl.when(end)
         def _():
             tok_b[j] = total.astype(bf)
-            a_copy(j).start()
+            if j < steps - direct:
+                a_copy(j).start()
+            else:
+                near_copy(j).start()
+                beyond_copy(j).start()
 
         @pl.when(middle)
         def _():
             tok_f[j] = total
+            if j >= steps - direct:
+                b_out[j] = tok_f[j, pl.ds(far_at, th), :].astype(bf)
+                b_copy(j).start()
 
     def pair_sum(j):
+        if j >= steps - direct:
+            return
+
         @pl.when(middle)
         def _():
             a_copy(j).wait_recv()
@@ -727,18 +758,24 @@
     def line_sum(j):
         @pl.when(middle)
         def _():
+            total = tok_f[j, pl.ds(own_at, th), :]
+            if j >= steps - direct:
+                near_copy(j).wait_recv()
+                beyond_copy(j).wait_recv()
+                total = total + a_in[j, 0:th, :].astype(f32) + a_in[j, th:tok, :].astype(f32)
             b_copy(j).wait_recv()
-            token_out[pl.ds(own_at, th), cols(core, j)] = (
-                tok_f[j, pl.ds(own_at, th), :] + b_in[j].astype(f32)
-            ).astype(bf)
+            token_out[pl.ds(own_at, th), cols(core, j)] = (total + b_in[j].astype(f32)).astype(bf)
             c_copy(j, own_at).start()
             e_copy(j, own_at).start()
+            if j >= steps - far:
+                far_copy(j, own_at).start()
 
     def relay(j):
         @pl.when(middle)
         def _():
             c_copy(j, far_at).wait_recv()
-            q_copy(j, far_at).start()
+            if j < steps - far:
+                q_copy(j, far_at).start()
             f_copy(j, core).start()
 
     def collect(j):
@@ -748,15 +785,15 @@
             q_copy(j, beyond_at).wait_recv()
             f_copy(j, core).start()
 
-    left = strips - strips // 2
     filler = {
-        i: [lambda i=i: loop_gate_up(strips // 2 + i * left // 3, strips // 2 + (i + 1) * left // 3)]
-        for i in range(3)
+        1: [lambda: loop_gate_up(strips // 2, strips - 1), work_score_b],
+        2: [lambda: loop_gate_up(strips - 1, strips), work_norm_a],
+        3: [lambda: down(0)],
+        4: [work_norm_b],
+        5: [lambda: down(1)],
+        steps + 1: [work_score_c],
+        steps + 2: [work_norm_c],
     }
-    filler[1].append(work_score_b)
-    filler[3] = [work_norm_a, lambda: down(0)]
-    filler[4] = [work_norm_b]
-    filler[5] = [lambda: down(1)]
     stages = (
         ("combine", 0, combine), ("pair_sum", lag_a, pair_sum), ("line_sum", lag_b, line_sum),
         ("relay", lag_c, relay), ("collect", lag_e, collect),
@@ -766,13 +803,12 @@
             if 0 <= s - lag < steps:
                 with jax.named_scope(name):
                     step(s - lag)
-        for item in filler.get(s, []):
-            with jax.named_scope("filler"):
-                item()
+            if lag == 0:
+                for item in filler.get(s, []):
+                    with jax.named_scope("filler"):
+                        item()
 
     with jax.named_scope("last"):
-        work_score_c()
-        work_norm_c()
         work_norm_d()
 
     with jax.named_scope("w_final"):
@@ -784,7 +820,11 @@
     @pl.when(end)
     def _():
         for j in range(steps):
-            a_copy(j).wait_send()
+            if j < steps - direct:
+                a_copy(j).wait_send()
+            else:
+                near_copy(j).wait_send()
+                beyond_copy(j).wait_send()
 
     @pl.when(middle)
     def _():
@@ -792,13 +832,17 @@
             b_copy(j).wait_send()
             c_copy(j, own_at).wait_send()
             e_copy(j, own_at).wait_send()
-            q_copy(j, far_at).wait_send()
+            if j < steps - far:
+                q_copy(j, far_at).wait_send()
+            else:
+                far_copy(j, own_at).wait_send()
 
     for lo, n in groups:
-        exchange(lo, n).wait_send()
-    for d in (1, 2):
-        back(d, 0).wait_send()
-        back(d, 1).wait_send()
+        exchange(lo, n, 0).wait_send()
+        exchange(lo, n, 1).wait_send()
+    for q in range(steps // 2):
+        back(1, q).wait_send()
+        back(2, q).wait_send()
     share(0, 0, 0, core).wait_send()
     for d, c, s in pieces:
         share(d, c, s, core).wait_send()
@@ -872,9 +916,9 @@
             vm((8, tok), f32), vm((8, tok), f32), vm((nz, 8, tok), f32), vm((8, tok), f32),
             vm((n_ep, 8, tok), f32),
             dma((7,)), dma((n_ep, 3)), dma((n_ep, 3)), dma((n_ep, 2)), dma((n_ep, 2)),
-            dma((n_ep, 5)), dma((n_ep, 5)), dma((n_ep,)), dma((n_ep,)),
+            dma((n_ep, 5)), dma((n_ep, 5)), dma((2 * n_ep,)), dma((2 * n_ep,)),
             dma((n_ep, steps)), dma((n_ep, steps)),
-        ] + [dma((steps,))] * 12 + [
+        ] + [dma((steps,))] * 14 + [
             dma, dma, dma((nz,)), dma((nz,)), dma, dma, dma, dma, dma((nz,)), dma((nz,)),
             dma((n_ep,)), dma((n_ep,)),
         ],

time: 81.4 us -> 73.2 us (0.90)
  Pallas kernels: 80.4 us -> 72.3 us
    pallas_call x1, Pallas kernels: 77.3 us -> 69.1 us  [fused(): pl.pallas_call(functools.partial(fused_kernel, n_ep, n_tp, cap), out_shap...]
where the time goes in v2:
time: 73.2 us; the launch traced here: 73.1 us
  Pallas kernels  72.3 us (99%)
  between operations  0.81 us (1%)
    pallas_call x1, Pallas kernels, fused(): pl.pallas_call(functools.partial(fused_kernel, n_ep, n_tp, cap), out_shap...  69.1 us
    pallas_call x1, Pallas kernels, fused(): pl.pallas_call(functools.partial(store_kernel, count), out_shape=shapes,...  3.14 us

profile of v2, /device:TPU:0, one launch (start us, length us, event | category | flops | bytes accessed | tf_op | source)
XLA Modules:
  0.0 73.1 jit_solution(18090493015458654771)
XLA Ops:
  0.6 69.1 %fused.1 = (bf16[256,2048]{1,0:T(8,128)(2,1)S(1)}, bf16[2048,512]{1,0:T(8,128)(2,1)S(1)}, bf16[2048,512]{1,0:T(8,128)(2,1)S(1)}, bf16[512,2048]{1,0:T(8,128)(2,1...) custom-call(bf16[256,2048]{1,0:T(8,128)(2,1)} %tok_ref.1, ...), custom_call_target="tpu_custom_call" | custom-call | tf_op jit(solution)/shard_map/fused/pallas_call | solution.py:899
  69.8 3.1 %store.1 = (bf16[256,2048]{1,0:T(8,128)(2,1)}, bf16[2048,512]{1,0:T(8,128)(2,1)}, bf16[2048,512]{1,0:T(8,128)(2,1)}, bf16[512,2048]{1,0:T(8,128)(2,1)}, f32[1,20...) custom-call(bf16[256,2048]{1,0:T(8,128)(2,1)S(1)} %get-tuple-element.27.refs_0_, ...), custom_call_target="tpu_custom_call" | custom-call | tf_op jit(solution)/shard_map/store/pallas_call | solution.py:933

commit v3 on v2

--- a/solution.py
+++ b/solution.py
@@ -248,10 +248,10 @@
     token_out, gate_g, up_g, down_g, gate_norm, up_norm, down_norm, prob_grad, group_grad,
     route_ref, group_ref, prob_ref, src_v, gate_v, up_v, down_v, mine, rows, gate_p, up_p, hid_p, pick_v, pick_t,
     part_out, part_in, part_own, part_sum, returned,
-    tok_f, tok_b, a_in, b_out, b_in,
+    early_in, tok_f, tok_b, a_in, b_out, b_in,
     norm_part, norm_in, norm_z, norm_fin, score_part, score_in, score_z, score_tot, score_ep,
     load_sem, sx, rx, zs, zr, fs, fr, ps, pr, es, er, a_s, a_r, b_s, b_r, c_s, c_r, e_s, e_r, q_s, q_r,
-    g_s, g_r, f_s, f_r, ns, nr, nzs, nzr, nfs, nfr, ss, sr, szs, szr, ses, ser,
+    f_s, f_r, p_s, p_r, ns, nr, nzs, nzr, nfs, nfr, ss, sr, szs, szr, ses, ser,
 ):
     bf, f32 = jnp.bfloat16, jnp.float32
     me = lax.axis_index("ep")
@@ -416,19 +416,40 @@
     jw = 128
     steps = half // jw
     groups = ((0, 1), (1, 2), (3, 1))
+    piece_at = (0, 1, 4, 5, 6, 7, 2, 3)
+    early = 2
+    early_q = piece_at[-1] // 2
+    early_cols = slice(early_q * 2 * jw, (early_q + 1) * 2 * jw)
+
+    def early_copy(d):
+        src = returned.at[0, :, early_cols] if d == 0 else part_sum.at[d - 1, :, early_cols]
+        return remote(src, early_in.at[d], p_s.at[d], p_r.at[d], {"tp": across})
+
+    def early_sum(ds):
+        @pl.when(middle)
+        def _():
+            for d in ds:
+                early_copy(d).wait_recv()
+                own = returned[0, :, early_cols] if d == 0 else part_sum[d - 1, :, early_cols]
+                total = (own.astype(f32) + early_in[d].astype(f32)).astype(bf)
+                if d == 0:
+                    returned[0, :, early_cols] = total
+                else:
+                    part_sum[d - 1, :, early_cols] = total
+                for n in (steps - 2, steps - 1) if d == 3 else (early_q,) if d else ():
+                    back(d, n).start()
 
     def back(d, j):
-        w = jw if d == 3 else 2 * jw
-        at = pl.ds(j * w, w)
+        at = pl.ds(piece_at[j] * jw, jw) if d == 3 else pl.ds(j * 2 * jw, 2 * jw)
         return remote(
             part_sum.at[d - 1, :, at], returned.at[d, :, at], es.at[d, j], er.at[d, j], {"ep": peers[d]}
         )
 
     replies = {
-        (3, 0): [(3, j) for j in range(steps // 2)],
-        (3, 1): [(3, j) for j in range(steps // 2, steps - 2)],
-        (1, 0): [(1, 0), (2, 0), (3, steps - 2), (1, 1), (2, 1), (3, steps - 1)],
-        (1, 1): [(d, q) for q in range(2, steps // 2) for d in (1, 2)],
+        (3, 0): [(3, 0), (3, 1)],
+        (3, 1): [(3, 2), (3, 3)],
+        (1, 0): [(1, 0), (2, 0), (3, 4)],
+        (1, 1): [(1, 2), (2, 2), (3, 5), (1, 3), (2, 3)],
     }
 
     def block(lo, count, between=()):
@@ -484,6 +505,11 @@
                         part_sum[lo + i - 1, :, n:n + 256] = piece
             for d, n in replies.get((lo, h), ()):
                 back(d, n).start()
+            if h == early_q // 2:
+                @pl.when(end)
+                def _():
+                    for d in range(lo, lo + count):
+                        early_copy(d).start()
 
     def arrive(d, c):
         to_peer(d, c).wait_recv()
@@ -531,7 +557,7 @@
     with jax.named_scope("w_sh12"):
         shared(1)
         shared(2)
-    block(1, 2)
+    block(1, 2, (lambda: early_sum((0, 3)),))
 
     def score_pair():
         return remote(score_part, score_in, ss, sr, {"tp": partner})
@@ -669,20 +695,12 @@
     far_at = pl.multiple_of((2 - z) * th, 128)
 
     def cols(c, j):
-        return pl.ds(pl.multiple_of(c * half + j * jw, 128), jw)
+        return pl.ds(pl.multiple_of(c * half + piece_at[j] * jw, 128), jw)
 
     far_end = lax.rem(t + n_tp // 2, n_tp)
-    direct, far = 1, 3
+    far = 3
     near_at = pl.multiple_of(jnp.where(z == 0, 0, th), 128)
     beyond_at = pl.multiple_of(jnp.where(z == 0, th, 0), 128)
-
-    def near_copy(j):
-        return remote(tok_b.at[j, pl.ds(near_at, th)], a_in.at[j, pl.ds(0, th)], a_s.at[j], a_r.at[j],
-                      {"tp": across})
-
-    def beyond_copy(j):
-        return remote(tok_b.at[j, pl.ds(beyond_at, th)], a_in.at[j, pl.ds(th, th)], g_s.at[j], g_r.at[j],
-                      {"tp": far_end})
 
     def a_copy(j):
         return remote(tok_b.at[j], a_in.at[j], a_s.at[j], a_r.at[j], {"tp": across})
@@ -714,34 +732,40 @@
     lag_a, lag_b, lag_c, lag_e = 1, 3, 5, steps
 
     def combine(j):
+        if j >= steps - early:
+            @pl.when(middle)
+            def _():
+                total = token_part(j)
+                tok_f[j] = total
+                b_out[j] = tok_f[j, pl.ds(far_at, th), :].astype(bf)
+                b_copy(j).start()
+
+            return
+        total = token_part(j)
+
+        @pl.when(end)
+        def _():
+            tok_b[j] = total.astype(bf)
+            a_copy(j).start()
+
+        @pl.when(middle)
+        def _():
+            tok_f[j] = total
+
+    def token_part(j):
         if j % 2 == 0:
-            back(1, j // 2).wait_recv()
-            back(2, j // 2).wait_recv()
+            back(1, piece_at[j] // 2).wait_recv()
+            back(2, piece_at[j] // 2).wait_recv()
         back(3, j).wait_recv()
-        at = slice(j * jw, (j + 1) * jw)
+        at = slice(piece_at[j] * jw, (piece_at[j] + 1) * jw)
         total = None
         for d in range(n_ep):
             more = jnp.dot(pick_t[d], returned[d, :, at], preferred_element_type=f32)
             total = more if total is None else total + more
-
-        @pl.when(end)
-        def _():
-            tok_b[j] = total.astype(bf)
-            if j < steps - direct:
-                a_copy(j).start()
-            else:
-                near_copy(j).start()
-                beyond_copy(j).start()
-
-        @pl.when(middle)
-        def _():
-            tok_f[j] = total
-            if j >= steps - direct:
-                b_out[j] = tok_f[j, pl.ds(far_at, th), :].astype(bf)
-                b_copy(j).start()
+        return total
 
     def pair_sum(j):
-        if j >= steps - direct:
+        if j >= steps - early:
             return
 
         @pl.when(middle)
@@ -759,10 +783,6 @@
         @pl.when(middle)
         def _():
             total = tok_f[j, pl.ds(own_at, th), :]
-            if j >= steps - direct:
-                near_copy(j).wait_recv()
-                beyond_copy(j).wait_recv()
-                total = total + a_in[j, 0:th, :].astype(f32) + a_in[j, th:tok, :].astype(f32)
             b_copy(j).wait_recv()
             token_out[pl.ds(own_at, th), cols(core, j)] = (total + b_in[j].astype(f32)).astype(bf)
             c_copy(j, own_at).start()
@@ -786,7 +806,7 @@
             f_copy(j, core).start()
 
     filler = {
-        1: [lambda: loop_gate_up(strips // 2, strips - 1), work_score_b],
+        1: [lambda: early_sum((1, 2)), lambda: loop_gate_up(strips // 2, strips - 1), work_score_b],
         2: [lambda: loop_gate_up(strips - 1, strips), work_norm_a],
         3: [lambda: down(0)],
         4: [work_norm_b],
@@ -815,16 +835,16 @@
         for j in range(steps):
             f_copy(j, 1 - core).wait_recv()
             f_copy(j, core).wait_send()
-            back(3, j).wait_send()
+            if j < steps - early:
+                back(3, j).wait_send()
 
     @pl.when(end)
     def _():
         for j in range(steps):
-            if j < steps - direct:
+            if j < steps - early:
                 a_copy(j).wait_send()
-            else:
-                near_copy(j).wait_send()
-                beyond_copy(j).wait_send()
+        for d in range(n_ep):
+            early_copy(d).wait_send()
 
     @pl.when(middle)
     def _():
@@ -841,8 +861,17 @@
         exchange(lo, n, 0).wait_send()
         exchange(lo, n, 1).wait_send()
     for q in range(steps // 2):
-        back(1, q).wait_send()
-        back(2, q).wait_send()
+        if q != early_q:
+            back(1, q).wait_send()
+            back(2, q).wait_send()
+
+    @pl.when(middle)
+    def _():
+        back(1, early_q).wait_send()
+        back(2, early_q).wait_send()
+        for j in range(steps - early, steps):
+            back(3, j).wait_send()
+
     share(0, 0, 0, core).wait_send()
     for d, c, s in pieces:
         share(d, c, s, core).wait_send()
@@ -909,6 +938,7 @@
             vm((n_ep, cap, tok), bf), vm((n_ep, tok, cap), bf),
             vm((slots, half), bf), vm((slots, half), bf), vm((2 * cap, half), f32),
             vm((n_ep - 1, cap, half), bf), vm((n_ep, cap, half), bf),
+            vm((n_ep, cap, 2 * jw), bf),
             vm((steps, tok, jw), f32), vm((steps, tok, jw), bf), vm((steps, tok, jw), bf),
             vm((steps, th, jw), bf), vm((steps, th, jw), bf),
             vm((2, width // 128, 128), f32), vm((width // 128, 128), f32),
@@ -918,7 +948,7 @@
             dma((7,)), dma((n_ep, 3)), dma((n_ep, 3)), dma((n_ep, 2)), dma((n_ep, 2)),
             dma((n_ep, 5)), dma((n_ep, 5)), dma((2 * n_ep,)), dma((2 * n_ep,)),
             dma((n_ep, steps)), dma((n_ep, steps)),
-        ] + [dma((steps,))] * 14 + [
+        ] + [dma((steps,))] * 12 + [dma((n_ep,)), dma((n_ep,))] + [
             dma, dma, dma((nz,)), dma((nz,)), dma, dma, dma, dma, dma((nz,)), dma((nz,)),
             dma((n_ep,)), dma((n_ep,)),
         ],

time: 73.2 us -> 72.9 us (level)
  no operation moved by 1% of the time
where the time goes in v3:
time: 72.9 us; the launch traced here: 72.8 us
  Pallas kernels  71.9 us (99%)
  between operations  0.81 us (1%)
    pallas_call x1, Pallas kernels, fused(): pl.pallas_call(functools.partial(fused_kernel, n_ep, n_tp, cap), out_shap...  68.8 us
    pallas_call x1, Pallas kernels, fused(): pl.pallas_call(functools.partial(store_kernel, count), out_shape=shapes,...  3.14 us

profile of v3, /device:TPU:0, one launch (start us, length us, event | category | flops | bytes accessed | tf_op | source)
XLA Modules:
  0.0 72.8 jit_solution(13323586678197329069)
XLA Ops:
  0.6 68.8 %fused.1 = (bf16[256,2048]{1,0:T(8,128)(2,1)S(1)}, bf16[2048,512]{1,0:T(8,128)(2,1)S(1)}, bf16[2048,512]{1,0:T(8,128)(2,1)S(1)}, bf16[512,2048]{1,0:T(8,128)(2,1...) custom-call(bf16[256,2048]{1,0:T(8,128)(2,1)} %tok_ref.1, ...), custom_call_target="tpu_custom_call" | custom-call | tf_op jit(solution)/shard_map/fused/pallas_call | solution.py:928
  69.5 3.1 %store.1 = (bf16[256,2048]{1,0:T(8,128)(2,1)}, bf16[2048,512]{1,0:T(8,128)(2,1)}, bf16[2048,512]{1,0:T(8,128)(2,1)}, bf16[512,2048]{1,0:T(8,128)(2,1)}, f32[1,20...) custom-call(bf16[256,2048]{1,0:T(8,128)(2,1)S(1)} %get-tuple-element.27.refs_0_, ...), custom_call_target="tpu_custom_call" | custom-call | tf_op jit(solution)/shard_map/store/pallas_call | solution.py:963
